TPU v7x, 256 devices: a 4x2x16 block of a 4x16x16 slice. The times are simulated.
256 devices in a mesh: grp: 2 (over y), ep: 32 (over z, core), tp: 4 (over x).
Axes of the slice: x: 4, y: 2, z: 16, core: 2. Of those that a mesh axis runs over, the one named last changes fastest.
The devices are a block of a 4x16x16 slice.
Arguments:
- tokens: bfloat16 [16384, 2048], P(('grp', 'ep', 'tp')), parts along dimension 0, may hold values from -6 to 6
- gain_in: float32 [2048], replicated, may hold values from 0.1 to 1.9
- routes: int32 [16384, 2], P(('grp', 'ep')), parts along dimension 0, may hold values from 0 to 31, all different within a row; in each aligned block of 64 rows (0 to 63, 64 to 127, ...) at most 6 rows name the same one
- gates: float32 [16384, 2], P(('grp', 'ep')), parts along dimension 0, may hold values from 0.05 to 1
- w_gate: bfloat16 [32, 2048, 3072], P('ep', None, 'tp'), may hold values from -0.125 to 0.125
- w_up: bfloat16 [32, 2048, 3072], P('ep', None, 'tp'), may hold values from -0.125 to 0.125
- w_down: bfloat16 [32, 3072, 2048], P('ep', 'tp'), may hold values from -0.109375 to 0.109375
- gain_out: float32 [2048], P('tp'), may hold values from 0.3 to 3
Outputs:
- mixed: bfloat16 [16384, 2048], P(('grp', 'ep'), 'tp'), parts along dimension 0
There are 2 independent parts, one for each index of `grp`. A program takes and returns all parts, laid end to end along the dimension named above; an argument that names none is the same for every part. Nothing has to cross between parts.
Inputs may be any that keep to these rules, and one draw needn't show every extreme that they name: `routes`: each row names 2 different experts; every expert is named by some row. Among the rows of one device (aligned blocks of 64 rows) no expert is named more than 6 times, and in every draw some expert is named exactly 6 times in some such block.
All inputs are finite; a program needn't handle non-finite values.
Results may differ from a plain program's by a relative error of at most 0.012.
Values may be sent and summed in bfloat16 or wider, within the bound.
No kernel may reach another device: no remote copies, remote signals or barrier semaphores. Data moves between devices by JAX's collectives and lax.ppermute only.
A program may use at most 64 MiB of HBM per device.

v0:
```python
import jax
import jax.numpy as jnp
from jax import lax
from jax.sharding import PartitionSpec as P

EPS = 1e-06


def from_everyone(shard, axis):
    size = lax.axis_size(axis)
    return lax.all_to_all(
        jnp.broadcast_to(shard[None], (size, *shard.shape)), axis, 0, 0, tiled=True
    )


def of_everyone(shard, axis):
    everything = from_everyone(shard, axis)
    return jnp.sum(everything, axis=0)


def slot_table(routes, experts, capacity):
    sources, count, choose = routes.shape
    flat = routes.reshape(sources, count * choose)
    onehot = (flat[:, :, None] == jnp.arange(experts, dtype=jnp.int32)[None, None, :]).astype(
        jnp.int32
    )
    earlier = jnp.cumsum(onehot, axis=1) - onehot
    slot = jnp.sum(earlier * onehot, axis=2)
    return (flat * capacity + slot).reshape(sources, count, choose)


def local(tokens, gain_in, routes, gates, w_gate, w_up, w_down, gain_out):
    count, width = tokens.shape
    choose = routes.shape[1]
    experts = lax.axis_size("ep")
    groups = lax.axis_size("tp")
    capacity = (3 * count * choose + 2 * experts - 1) // (2 * experts)
    hidden_width = w_gate.shape[2]
    values = tokens.astype(jnp.float32)
    normed = (
        values * lax.rsqrt(jnp.mean(values * values, axis=-1, keepdims=True) + EPS) * gain_in
    ).astype(jnp.bfloat16)
    positions = slot_table(routes.reshape(groups, count, choose), experts, capacity)
    own = lax.dynamic_index_in_dim(positions, lax.axis_index("tp"), 0, keepdims=False)
    slots = jnp.arange(experts * capacity, dtype=jnp.int32)
    select = jnp.sum((own[None, :, :] == slots[:, None, None]).astype(jnp.bfloat16), axis=2)
    outgoing = jnp.dot(select, normed, preferred_element_type=jnp.float32).astype(jnp.bfloat16)
    outgoing = outgoing.reshape(experts, capacity, width)
    arrived = lax.all_to_all(outgoing, "ep", split_axis=0, concat_axis=0, tiled=True)
    piece = lax.all_gather(arrived[:, None], "tp", axis=1, tiled=True)
    flat = piece.reshape(-1, width)
    gate = jnp.dot(flat, w_gate[0], preferred_element_type=jnp.float32)
    up = jnp.dot(flat, w_up[0], preferred_element_type=jnp.float32)
    hidden = (jax.nn.silu(gate) * up).astype(jnp.bfloat16)
    hidden = hidden.reshape(piece.shape[:-1] + (hidden_width,))
    partial_value = jnp.dot(
        hidden.reshape(-1, hidden_width), w_down[0], preferred_element_type=jnp.float32
    )
    summed = lax.psum_scatter(
        partial_value.astype(jnp.bfloat16), "tp", scatter_dimension=1, tiled=True
    )
    slice_width = width // groups
    expert_out = summed.reshape(experts, groups * capacity, slice_width)
    returned = lax.all_to_all(expert_out, "ep", split_axis=0, concat_axis=0, tiled=True)
    returned = returned.reshape(experts, groups, capacity, slice_width).transpose(1, 0, 2, 3)
    returned = returned.reshape(groups, experts * capacity, slice_width).astype(jnp.float32)
    weights = gates.reshape(groups, count, choose)
    combine = jnp.sum(
        jnp.where(
            positions[..., None] == slots[None, None, None, :], weights[..., None], jnp.float32(0.0)
        ),
        axis=2,
    )
    combined = jnp.einsum("gtp,gpd->gtd", combine, returned)
    combined = combined.reshape(groups * count, slice_width)
    squares = of_everyone(jnp.sum(combined * combined, axis=1), "tp")
    scale = lax.rsqrt(squares / width + EPS)
    return (combined * scale[:, None] * gain_out).astype(jnp.bfloat16)


def solution(mesh):
    in_specs = (
        P(("grp", "ep", "tp"), None),
        P(),
        P(("grp", "ep"), None),
        P(("grp", "ep"), None),
        P("ep", None, "tp"),
        P("ep", None, "tp"),
        P("ep", "tp", None),
        P("tp"),
    )
    out_specs = P(("grp", "ep"), "tp")
    return jax.shard_map(local, mesh=mesh, in_specs=in_specs, out_specs=out_specs, check_vma=False)
```

profile of v0, /device:TPU:33, one launch (start us, length us, event | category | flops | bytes accessed | tf_op | source)
XLA Modules:
  0.0 278.8 jit_solution(4888810411502820431)
XLA Ops:
  6.6 1.0 copy.61
  7.5 0.7 broadcast_multiply_fusion
  8.2 0.1 eq.43
  8.3 0.8 fusion.19
  9.2 1.2 reduce_window_sum.11
  10.4 0.2 select_reduce_fusion.1
  10.7 0.1 copy.62
  10.8 0.1 copy.63
  10.9 0.1 mul.65
  11.0 0.1 fusion.21
  11.1 1.1 fusion.11
  12.2 2.3 convolution_convert_fusion.1
  14.5 2.2 reshape.60
  16.7 80.9 %all_to_all.16 = bf16[32,6,2048]{2,1,0:T(8,128)(2,1)S(1)} all-to-all(bf16[32,6,2048]{2,1,0:T(8,128)(2,1)} %reshape.60), channel_id=1, replica_groups=mesh['grp'=2,'ep'=32,'tp'=4] {'ep'}, dimensions={0} | all-to-all | bytes 1572864 | tf_op jit(solution)/shard_map/all_to_all | solution.py:49
  97.6 1.3 copy.66
  99.0 0.1 reduce-scatter.2.cloned.1.call-start
  99.1 38.0 %all-gather.3.cloned.1.call-done = bf16[32,24,2048]{2,0,1:T(8,128)(2,1)} async-done(((bf16[32,6,2048]{2,0,1:T(8,128)(2,1)}), bf16[32,24,2048]{2,0,1:T(8,128)(2,1)}) %all-gather.3.cloned.1.call-update) | async-done | bytes 3145744 | tf_op jit(solution)/shard_map/all_gather | solution.py:50
  137.1 3.8 %copy.67 = bf16[32,24,2048]{2,1,0:T(8,128)(2,1)S(1)} copy(bf16[32,24,2048]{2,0,1:T(8,128)(2,1)} %all-gather.3.cloned.1.call-done) | data formatting | bytes 6291456 | tf_op jit(solution)/shard_map/all_gather | solution.py:50
  140.9 1.7 copy-done.1
  142.6 4.0 %fusion.1 = f32[768,768]{1,0:T(8,128)} fusion(bf16[768,2048]{1,0:T(8,128)(2,1)S(1)} %bitcast.35, bf16[1,2048,768]{2,1,0:T(8,128)(2,1)S(1)} %copy-done.4), kind=kOutput, calls=%fused_computation.2 | convolution fusion | flops 2415919104 | bytes 8650752 | tf_op jit(solution)/shard_map/dot_general | solution.py:53
  146.6 11.0 %convolution_convert_fusion = bf16[768,2048]{1,0:T(8,128)(2,1)} fusion(bf16[1,768,2048]{2,1,0:T(8,128)(2,1)S(1)} %copy-done, f32[768,768]{1,0:T(8,128)} %fusion.1, bf16[768,2048]{1,0:T(8,128)(2,1)} %bitcast.36, bf16[1,2048,768]{2,1,0:T(8,128)(2,1)} %param.12), kind=kOutput, calls=%fused_computation | convolution fusion | flops 4836950016 | bytes 14942208 | tf_op jit(solution)/shard_map/dot_general | solution.py:56
  157.7 44.8 %reduce-scatter.2.cloned.1.call-done = bf16[768,512]{1,0:T(8,128)(2,1)} async-done(((bf16[768,2048]{1,0:T(8,128)(2,1)}), bf16[768,512]{1,0:T(8,128)(2,1)}) %reduce-scatter.2.cloned.1.call-update) | async-done | bytes 786448 | tf_op jit(solution)/shard_map/reduce_scatter | solution.py:59
  202.5 13.3 %all-to-all-start.1 = ((bf16[32,24,512]{2,1,0:T(8,128)(2,1)}), bf16[32,24,512]{2,1,0:T(8,128)(2,1)}, u32[]{:S(2)}, u32[]{:S(2)}) async-start(bf16[32,24,512]{2,1,0:T(8,128)(2,1)} %bitcast.39), calls=%async_computation.2 | async-start | bytes 1572864 | tf_op jit(solution)/shard_map/all_to_all | solution.py:64
  215.8 0.1 broadcast_in_dim.20
  215.9 0.2 select_reduce_fusion
  216.1 44.2 %all-to-all-done.1 = bf16[32,24,512]{2,1,0:T(8,128)(2,1)} async-done(((bf16[32,24,512]{2,1,0:T(8,128)(2,1)}), bf16[32,24,512]{2,1,0:T(8,128)(2,1)}, u32[]{:S(2)}, u32[]{:S(2)}) %all-to-all-start.1) | async-done | bytes 786464 | tf_op jit(solution)/shard_map/all_to_all | solution.py:64
  260.3 1.4 copy.68
  261.7 0.6 copy.69
  262.3 1.1 multiply_reduce_fusion
  263.4 0.1 broadcast_in_dim.37
  263.5 6.5 %all_to_all.17 = f32[4,1,256]{2,1,0:T(1,128)S(1)} all-to-all(f32[4,1,256]{2,1,0:T(1,128)S(1)} %broadcast_in_dim.38), channel_id=1, replica_groups=mesh['grp'=2,'ep'=32,'tp'=4] {'tp'}, dimensions={0} | all-to-all | bytes 8192 | tf_op jit(solution)/shard_map/all_to_all | solution.py:11
  270.1 1.9 fusion.15
  (20 shorter events, 0.2 us)
Async XLA Ops:
  6.5 140.1 %copy-start = (bf16[1,768,2048]{2,1,0:T(8,128)(2,1)S(1)}, bf16[1,768,2048]{2,1,0:T(8,128)(2,1)}, u32[]{:S(2)}) copy-start(bf16[1,768,2048]{2,1,0:T(8,128)(2,1)} %param.14) | copy-start | bytes 9437188
  6.6 130.6 %all-gather.3.cloned.1.call-start = ((), (), s32[]{:S(2)}) async-start(), calls=%async_computation.5 | async-start | bytes 3932160 | tf_op jit(solution)/shard_map/all_gather | solution.py:50
  99.0 103.5 %reduce-scatter.2.cloned.1.call-start = ((), (), s32[]{:S(2)}) async-start(), calls=%async_computation.4 | async-start | bytes 3932160 | tf_op jit(solution)/shard_map/reduce_scatter | solution.py:59
  137.1 5.5 %copy-start.4 = (bf16[1,2048,768]{2,1,0:T(8,128)(2,1)S(1)}, bf16[1,2048,768]{2,1,0:T(8,128)(2,1)}, u32[]{:S(2)}) copy-start(bf16[1,2048,768]{2,1,0:T(8,128)(2,1)} %param.13) | copy-start | bytes 9437188
  140.9 1.7 copy-start.1
  157.6 58.2 %copy-start.3 = (f32[256,2]{0,1:T(2,128)S(1)}, f32[256,2]{0,1:T(2,128)}, u32[]{:S(2)}) copy-start(f32[256,2]{0,1:T(2,128)} %param.11) | copy-start | bytes 6148
  202.5 67.6 %copy-start.2 = (f32[512]{0:T(512)S(1)}, f32[512]{0:T(512)}, u32[]{:S(2)}) copy-start(f32[512]{0:T(512)} %param.15) | copy-start | bytes 6148
  202.5 57.8 %all-to-all-start.1 = ((bf16[32,24,512]{2,1,0:T(8,128)(2,1)}), bf16[32,24,512]{2,1,0:T(8,128)(2,1)}, u32[]{:S(2)}, u32[]{:S(2)}) async-start(bf16[32,24,512]{2,1,0:T(8,128)(2,1)} %bitcast.39), calls=%async_computation.2 | async-start | bytes 1572864 | tf_op jit(solution)/shard_map/all_to_all | solution.py:64
Sparse Core Ops, SparseCore 0:
  99.1 37.9 all-gather.2
  157.8 44.6 reduce-scatter.1
where the time goes:
time: 279 us
  waiting for transfers between devices  127 us (46%)
  blocking collectives  87.4 us (31%)
  matrix products  18.5 us (7%)
  between operations  13.5 us (5%)
  starting transfers between devices  13.4 us (5%)
  local copies, waits for them, and re-layouts  12.5 us (4%)
  other arithmetic  6.3 us (2%)
    all_to_all x1, blocking collectives, local(): lax.all_to_all(outgoing, 'ep', split_axis=0, concat_axis=0, tiled=True)  80.9 us
    reduce_scatter x1, waiting for transfers between devices, local(): lax.psum_scatter(partial_value.astype(jnp.bfloat16), 'tp', scatter_dimens...  44.8 us
    all_to_all x1, waiting for transfers between devices, local(): lax.all_to_all(expert_out, 'ep', split_axis=0, concat_axis=0, tiled=True)  44.2 us
    all_gather x1, waiting for transfers between devices, local(): piece = lax.all_gather(arrived[:, None], 'tp', axis=1, tiled=True)  38 us
    all_to_all x1, starting transfers between devices, local(): lax.all_to_all(expert_out, 'ep', split_axis=0, concat_axis=0, tiled=True)  13.3 us
    dot_general x1, matrix products, local(): jnp.dot(hidden.reshape(-1, hidden_width), w_down[0], preferred_element_ty...  11 us
    all_to_all x1, blocking collectives, from_everyone(): lax.all_to_all(jnp.broadcast_to(shard[None], (size, *shard.shape)), axis,...  6.5 us
  transfers between devices with their start and end apart: 3, of which 3 were waited for; matrix products, arithmetic and copies ran while one was open for 0% of the time, Pallas kernels for 0%

commit v1 on v0

v1 whole, which is shorter than its diff:
```python
import functools

import jax
import jax.numpy as jnp
from jax import lax
from jax.experimental import pallas as pl
from jax.experimental.pallas import tpu as pltpu
from jax.sharding import PartitionSpec as P


EPS = 1e-06
CHUNKS = 2
TILE = 256
NARROW = jnp.bfloat16
WIDE = jnp.float32
VMEM_LIMIT = 48 * 1024 * 1024


def rotate(value, axis, step):
    size = lax.axis_size(axis)
    return lax.ppermute(value, axis, [(i, (i + step) % size) for i in range(size)])


def partner(value):
    return lax.ppermute(value, "ep", [(i, i ^ 1) for i in range(lax.axis_size("ep"))])


def exchange(value):
    size = lax.axis_size("ep")
    same = [list(range(core, size, 2)) for core in range(2)]
    return lax.all_to_all(value, "ep", 0, 0, tiled=True, axis_index_groups=same)


def dot(a, b):
    return jnp.dot(a, b, preferred_element_type=WIDE)


def one_hot(matches):
    return jnp.where(matches, 1.0, 0.0).astype(NARROW)


def places(own, other, capacity, span):
    both = jnp.concatenate([own * capacity, other * capacity + span], axis=0)
    column = jnp.concatenate([both[:, c : c + 1] for c in range(both.shape[1])], axis=0)
    total = column.shape[0]
    i = lax.broadcasted_iota(jnp.int32, (total, total), 0)
    j = lax.broadcasted_iota(jnp.int32, (total, total), 1)
    row = jnp.sum(jnp.where(i == j, column, 0), axis=0, keepdims=True)
    same = column == row
    row_slot = jnp.sum(jnp.where(same & (i < j), 1, 0), axis=0, keepdims=True)
    column_slot = jnp.sum(jnp.where(same & (j < i), 1, 0), axis=1, keepdims=True)
    return column + column_slot, row + row_slot


def pack_kernel(own, other, gain, own_routes, other_routes, row_key, *outs, capacity, span, groups):
    values = jnp.concatenate([own[...], other[...]], axis=0).astype(WIDE)
    scale = lax.rsqrt(jnp.mean(values * values, axis=-1, keepdims=True) + EPS)
    normed = (values * scale * gain[...]).astype(NARROW)
    _, row = places(own_routes[...], other_routes[...], capacity, span)
    rows = values.shape[0]
    lanes = values.shape[1] // groups
    for k, out in enumerate(outs):
        key = row_key[...] + k * (capacity // len(outs))
        total = None
        for q in range(groups):
            hit = key == row[:, :rows] + q * 2 * span
            for c in range(1, row.shape[1] // rows):
                hit = hit | (key == row[:, c * rows : (c + 1) * rows] + q * 2 * span)
            piece = dot(one_hot(hit), normed[:, q * lanes : (q + 1) * lanes])
            total = piece if total is None else total + piece
        out[...] = total.astype(NARROW)


def spread_kernel(arrived, line_row, out, *, groups):
    lanes = arrived.shape[1]
    column = lax.broadcasted_iota(jnp.int32, (line_row.shape[0], arrived.shape[0]), 1)
    for q in range(groups):
        pick = one_hot(line_row[...] + q == column)
        out[:, q * lanes : (q + 1) * lanes] = dot(pick, arrived[...]).astype(NARROW)


def expert_kernel(*refs):
    sources, (wg, wu, wd), sinks, (flat, acc) = refs[:5], refs[5:8], refs[8:13], refs[13:]
    step = pl.program_id(0)

    @pl.when(step == 0)
    def _():
        at = 0
        for source in sources:
            flat[at : at + source.shape[0], :] = source[...]
            at += source.shape[0]

    gate = dot(flat[...], wg[0])
    up = dot(flat[...], wu[0])
    hidden = (gate / (1.0 + jnp.exp(-gate)) * up).astype(NARROW)
    down = dot(hidden, wd[0])

    @pl.when(step == 0)
    def _():
        acc[...] = down

    @pl.when(step > 0)
    def _():
        acc[...] += down

    @pl.when(step == pl.num_programs(0) - 1)
    def _():
        at = 0
        for sink in sinks:
            sink[...] = acc[at : at + sink.shape[0], :].astype(sink.dtype)
            at += sink.shape[0]


def leave_kernel(kept, got, back, out, *, groups):
    both = jnp.concatenate([kept[...], got[...]], axis=0)
    lanes = both.shape[1] // groups
    column = lax.broadcasted_iota(jnp.int32, (out.shape[0], both.shape[0]), 1)
    total = None
    for q in range(groups):
        pick = one_hot(back[...] == column + q * both.shape[0])
        piece = dot(pick, both[:, q * lanes : (q + 1) * lanes])
        total = piece if total is None else total + piece
    out[...] = total.astype(NARROW)


def finish_kernel(*refs, capacity, span, groups):
    returned = refs[:CHUNKS]
    own_routes, other_routes, gates, column_key, quarters = refs[CHUNKS : CHUNKS + 5]
    gains = refs[CHUNKS + 5 : CHUNKS + 5 + groups]
    outs = refs[CHUNKS + 5 + groups :]
    column, _ = places(own_routes[...], other_routes[...], capacity, span)
    count, choose = gates.shape
    width = groups * returned[0].shape[1]
    total = None
    for k in range(CHUNKS):
        key = column_key[...] + k * (capacity // CHUNKS)
        blocks = []
        for step in range(groups):
            weight = 0.0
            for c in range(choose):
                place = column[2 * c * count : (2 * c + 1) * count, :] + quarters[step]
                weight = weight + jnp.where(place == key, gates[:, c : c + 1], 0.0)
            blocks.append(weight)
        weight = jnp.concatenate(blocks, axis=0)
        high = weight.astype(NARROW)
        low = (weight - high.astype(WIDE)).astype(NARROW)
        piece = dot(high, returned[k][...]) + dot(low, returned[k][...])
        total = piece if total is None else total + piece
    squares = 0.0
    for step in range(groups):
        block = total[step * count : (step + 1) * count, :]
        squares = squares + jnp.sum(block * block, axis=1, keepdims=True)
    scale = lax.rsqrt(squares / width + EPS)
    for step in range(groups):
        block = total[step * count : (step + 1) * count, :]
        outs[step][...] = (block * scale * gains[step][...]).astype(NARROW)


def whole(spec):
    return jax.ShapeDtypeStruct(spec[0], spec[1])


def call(kernel, outs, *args, flops=0, moved=0, smem=(), **kwargs):
    return pl.pallas_call(
        functools.partial(kernel, **kwargs),
        out_shape=[whole(o) for o in outs],
        in_specs=[
            pl.BlockSpec(memory_space=pltpu.SMEM if i in smem else pltpu.VMEM)
            for i in range(len(args))
        ],
        out_specs=[pl.BlockSpec(memory_space=pltpu.VMEM) for _ in outs],
        cost_estimate=pl.CostEstimate(flops=flops, bytes_accessed=moved, transcendentals=0),
        compiler_params=pltpu.CompilerParams(vmem_limit_bytes=VMEM_LIMIT),
    )(*args)


def expert(sources, w_gate, w_up, w_down):
    _, width = sources[0].shape
    hidden = w_gate.shape[2]
    total = sum(s.shape[0] for s in sources)
    dtypes = [WIDE] + [NARROW] * (len(sources) - 1)
    fixed = lambda s: pl.BlockSpec(s.shape, lambda j: (0, 0))
    return pl.pallas_call(
        expert_kernel,
        grid=(hidden // TILE,),
        out_shape=[jax.ShapeDtypeStruct(s.shape, d) for s, d in zip(sources, dtypes)],
        in_specs=[fixed(s) for s in sources]
        + [
            pl.BlockSpec((1, width, TILE), lambda j: (0, 0, j)),
            pl.BlockSpec((1, width, TILE), lambda j: (0, 0, j)),
            pl.BlockSpec((1, TILE, width), lambda j: (0, j, 0)),
        ],
        out_specs=[fixed(s) for s in sources],
        scratch_shapes=[pltpu.VMEM((total, width), NARROW), pltpu.VMEM((total, width), WIDE)],
        cost_estimate=pl.CostEstimate(
            flops=6 * total * width * hidden,
            bytes_accessed=6 * width * hidden + 8 * total * width,
            transcendentals=total * hidden,
        ),
        compiler_params=pltpu.CompilerParams(
            dimension_semantics=("arbitrary",), vmem_limit_bytes=VMEM_LIMIT
        ),
    )(*sources, w_gate, w_up, w_down)


def gather_blocks(own):
    half = own.shape[0] // 2
    before = rotate(own, "tp", 1)
    after = rotate(own, "tp", -1)
    return [
        own,
        after,
        rotate(before[:half], "tp", 1),
        rotate(after[half:], "tp", -1),
        before,
    ]


def scatter_blocks(blocks):
    own, up, far_low, far_high, down = blocks
    half = own.shape[0] // 2
    from_before = rotate(far_low, "tp", 1)
    from_after = rotate(far_high, "tp", -1)
    up = jnp.concatenate(
        [(up[:half].astype(WIDE) + from_before.astype(WIDE)).astype(NARROW), up[half:]], axis=0
    )
    down = jnp.concatenate(
        [down[:half], (down[half:].astype(WIDE) + from_after.astype(WIDE)).astype(NARROW)], axis=0
    )
    up = rotate(up, "tp", 1).astype(WIDE)
    down = rotate(down, "tp", -1).astype(WIDE)
    return [
        (own[p] + up[p] + down[p]).astype(NARROW) for p in (slice(0, half), slice(half, None))
    ]


def local(tokens, gain_in, routes, gates, w_gate, w_up, w_down, gain_out):
    count, width = tokens.shape
    choose = routes.shape[1]
    experts = lax.axis_size("ep")
    groups = lax.axis_size("tp")
    chips = experts // 2
    capacity = (3 * count * choose + 2 * experts - 1) // (2 * experts)
    span = experts * capacity
    part = capacity // CHUNKS
    lanes = width // groups
    rows = chips * 2 * part * groups
    block = chips * 2 * part
    me = lax.axis_index("tp")
    core = lax.axis_index("ep") % 2

    own_routes = lax.dynamic_slice_in_dim(routes, me * count, count, 0)
    own_gates = lax.dynamic_slice_in_dim(gates, me * count, count, 0)
    other_routes = partner(own_routes)
    other_tokens = partner(tokens)

    row = jnp.arange(rows, dtype=jnp.int32)[:, None]
    quarter = row % groups
    slot = (row // groups) % part
    side = (row // (groups * part)) % 2
    chip = row // (groups * part * 2)
    row_key = (quarter * 2 + side) * span + (2 * chip + core) * capacity + slot
    column_key = (quarter * span + (2 * chip + (core ^ side)) * capacity + slot).reshape(1, rows)
    back = quarter * block + (side * chips + chip) * part + slot
    line = jnp.arange(block, dtype=jnp.int32)[:, None]
    line_row = ((line // part) % chips * 2 + line // (part * chips)) * part + line % part
    line_row = line_row * groups
    quarters = (me + jnp.arange(groups, dtype=jnp.int32)) % groups * span

    outgoing = call(
        pack_kernel,
        [((rows, lanes), NARROW)] * CHUNKS,
        tokens,
        other_tokens,
        gain_in[None],
        own_routes,
        other_routes,
        row_key,
        capacity=capacity,
        span=span,
        groups=groups,
        flops=2 * CHUNKS * rows * 2 * count * width,
        moved=4 * count * width,
    )
    arrived = []
    for k in range(CHUNKS):
        arrived.append(exchange(outgoing[k].reshape(chips, -1, lanes)).reshape(rows, lanes))
    gains = [gain_out[None]]
    gains += [rotate(gain_out[None], "tp", -step) for step in range(1, groups)]

    returned = []
    for k in range(CHUNKS):
        (own,) = call(
            spread_kernel,
            [((block, width), NARROW)],
            arrived[k],
            line_row,
            groups=groups,
            flops=2 * block * rows * width,
            moved=4 * block * width,
        )
        sources = gather_blocks(own)
        parts = expert(sources, w_gate, w_up, w_down)
        kept, sent = scatter_blocks(parts)
        got = partner(sent)
        (leaving,) = call(
            leave_kernel,
            [((rows, lanes), NARROW)],
            kept,
            got,
            back,
            groups=groups,
            flops=2 * rows * block * width,
            moved=4 * block * width,
        )
        returned.append(exchange(leaving.reshape(chips, -1, lanes)).reshape(rows, lanes))

    final = call(
        finish_kernel,
        [((count, lanes), NARROW)] * groups,
        *returned,
        own_routes,
        other_routes,
        own_gates,
        column_key,
        quarters,
        *gains,
        smem=(CHUNKS + 4,),
        capacity=capacity,
        span=span,
        groups=groups,
        flops=4 * CHUNKS * rows * groups * count * lanes,
        moved=4 * rows * lanes,
    )
    final = [final[0]] + [rotate(final[step], "tp", step) for step in range(1, groups)]
    out = []
    for j in range(groups):
        piece = final[0]
        for step in range(1, groups):
            piece = jnp.where((me - step) % groups == j, final[step], piece)
        out.append(piece)
    return jnp.concatenate(out, axis=0)


def solution(mesh):
    in_specs = (
        P(("grp", "ep", "tp"), None),
        P(),
        P(("grp", "ep"), None),
        P(("grp", "ep"), None),
        P("ep", None, "tp"),
        P("ep", None, "tp"),
        P("ep", "tp", None),
        P("tp"),
    )
    out_specs = P(("grp", "ep"), "tp")
    return jax.shard_map(local, mesh=mesh, in_specs=in_specs, out_specs=out_specs, check_vma=False)
```

time: 279 us -> 211 us (0.76)
  the two profiles are of different devices: /device:TPU:33 before, /device:TPU:40 now
where the time goes in v1:
time: 211 us
  waiting for transfers between devices  74 us (35%)
  starting transfers between devices  61.4 us (29%)
  blocking collectives  47.9 us (23%)
  Pallas kernels  21.9 us (10%)
  local copies, waits for them, and re-layouts  2.78 us (1%)
  other arithmetic  2.16 us (1%)
    all_to_all x1, blocking collectives, exchange(): return lax.all_to_all(value, 'ep', 0, 0, tiled=True, axis_index_groups=same)  47.9 us
    all_to_all x3, waiting for transfers between devices, exchange(): return lax.all_to_all(value, 'ep', 0, 0, tiled=True, axis_index_groups=same)  44.5 us
    ppermute x22, starting transfers between devices, rotate(): lax.ppermute(value, axis, [(i, (i + step) % size) for i in range(size)])  37.6 us
    ppermute x22, waiting for transfers between devices, rotate(): lax.ppermute(value, axis, [(i, (i + step) % size) for i in range(size)])  26 us
    all_to_all x3, starting transfers between devices, exchange(): return lax.all_to_all(value, 'ep', 0, 0, tiled=True, axis_index_groups=same)  23.5 us
    pallas_call x2, Pallas kernels, expert(): pl.pallas_call(expert_kernel, grid=(hidden // TILE,), out_shape=[jax.Shap...  15 us
    pallas_call x6, Pallas kernels, call(): pl.pallas_call(functools.partial(kernel, **kwargs), out_shape=[whole(o) f...  6.95 us
  transfers between devices with their start and end apart: 29, of which 14 were waited for; matrix products, arithmetic and copies ran while one was open for 1% of the time, Pallas kernels for 9%

profile of v1, /device:TPU:40, one launch (start us, length us, event | category | flops | bytes accessed | tf_op | source)
XLA Modules:
  0.0 210.6 jit_solution(18251353384711041033)
XLA Ops:
  3.8 1.6 shard_map.82
  5.3 47.9 %all_to_all.20 = bf16[16,24,512]{2,1,0:T(8,128)(2,1)S(1)} all-to-all(bf16[16,24,512]{2,1,0:T(8,128)(2,1)S(1)} %bitcast.14), channel_id=1, replica_groups={{0,8,16,24,32,40,48,56,64,72,80,88,96,104,112,120},{4,12,20,28,36,44,52..., dimensions={0} | all-to-all | bytes 786432 | tf_op jit(solution)/shard_map/all_to_all | solution.py:31
  53.2 6.0 %all-to-all-start = ((bf16[16,24,512]{2,1,0:T(8,128)(2,1)}), bf16[16,24,512]{2,1,0:T(8,128)(2,1)S(1)}, u32[]{:S(2)}, u32[]{:S(2)}) async-start(bf16[16,24,512]{2,1,0:T(8,128)(2,1)} %bitcast.1), calls=%async_computation | async-start | bytes 786432 | tf_op jit(solution)/shard_map/all_to_all | solution.py:31
  59.7 1.7 collective-permute-start.12
  61.5 1.7 collective-permute-start.11
  63.2 20.0 %all-to-all-done = bf16[16,24,512]{2,1,0:T(8,128)(2,1)S(1)} async-done(((bf16[16,24,512]{2,1,0:T(8,128)(2,1)}), bf16[16,24,512]{2,1,0:T(8,128)(2,1)S(1)}, u32[]{:S(2)}, u32[]{:S(2)}) %all-to-all-start) | async-done | bytes 393248 | tf_op jit(solution)/shard_map/all_to_all | solution.py:31
  83.6 1.7 collective-permute-start.3
  85.3 1.7 collective-permute-start.2
  87.5 3.0 %collective-permute-start.14 = (bf16[48,2048]{1,0:T(8,128)(2,1)S(1)}, bf16[48,2048]{1,0:T(8,128)(2,1)S(1)}, u32[]{:S(2)}, u32[]{:S(2)}) collective-permute-start(bf16[48,2048]{1,0:T(8,128)(2,1)S(1)} %slice.103), channel_id=1, source_target_pairs={{0,3},{1,0},{2,1},{3,2},{4,7},{5,4},{6,5},{7,6},{8,11},{9,8},{10,9... | collective-permute-start | bytes 589832 | tf_op jit(solution)/shard_map/ppermute | solution.py:21
  90.8 4.1 %collective-permute-done.3.refs_4_ = bf16[96,2048]{1,0:T(8,128)(2,1)S(1)} collective-permute-done((bf16[96,2048]{1,0:T(8,128)(2,1)S(1)}, bf16[96,2048]{1,0:T(8,128)(2,1)S(1)}, u32[]{:S(2)}, u32[]{:S(2)}) %collective-permute-start.3) | collective-permute-done | bytes 393248 | tf_op jit(solution)/shard_map/ppermute | solution.py:21
  95.0 3.5 %collective-permute-start.5 = (bf16[48,2048]{1,0:T(8,128)(2,1)S(1)}, bf16[48,2048]{1,0:T(8,128)(2,1)S(1)}, u32[]{:S(2)}, u32[]{:S(2)}) collective-permute-start(bf16[48,2048]{1,0:T(8,128)(2,1)S(1)} %slice.97), channel_id=1, source_target_pairs={{0,3},{1,0},{2,1},{3,2},{4,7},{5,4},{6,5},{7,6},{8,11},{9,8},{10,9... | collective-permute-start | bytes 589832 | tf_op jit(solution)/shard_map/ppermute | solution.py:21
  98.5 7.5 %shard_map.87 = (f32[96,2048]{1,0:T(8,128)S(1)}, bf16[96,2048]{1,0:T(8,128)(2,1)S(1)}, bf16[48,2048]{1,0:T(8,128)(2,1)S(1)}, bf16[48,2048]{1,0:T(8,128)(2,1)S(1)}, bf16[96,2048]{1,0:T(8,128)(2,1)S(1)}) custom-call(bf16[96,2048]{1,0:T(8,128)(2,1)S(1)} %shard_map.86.refs_0_, bf16[96,2048]{1,0:T(8,128)(2,1)S(1)} %collective-permute-done.11.refs_1_, ...), custom_call_target="tpu_custom_call" | custom-call | flops 3623878656 | bytes 15728640 | tf_op jit(solution)/shard_map/pallas_call | solution.py:183
  106.1 3.3 %collective-permute-start.17 = (bf16[48,2048]{1,0:T(8,128)(2,1)S(1)}, bf16[48,2048]{1,0:T(8,128)(2,1)S(1)}, u32[]{:S(2)}, u32[]{:S(2)}) collective-permute-start(bf16[48,2048]{1,0:T(8,128)(2,1)S(1)} %get-tuple-element.32), channel_id=1, source_target_pairs={{0,3},{1,0},{2,1},{3,2},{4,7},{5,4},{6,5},{7,6},{8,11},{9,8},{10,9... | collective-permute-start | bytes 589832 | tf_op jit(solution)/shard_map/ppermute | solution.py:21
  109.5 7.5 %shard_map.84 = (f32[96,2048]{1,0:T(8,128)S(1)}, bf16[96,2048]{1,0:T(8,128)(2,1)S(1)}, bf16[48,2048]{1,0:T(8,128)(2,1)S(1)}, bf16[48,2048]{1,0:T(8,128)(2,1)S(1)}, bf16[96,2048]{1,0:T(8,128)(2,1)S(1)}) custom-call(bf16[96,2048]{1,0:T(8,128)(2,1)S(1)} %shard_map.83.refs_0_, bf16[96,2048]{1,0:T(8,128)(2,1)S(1)} %collective-permute-done.2.refs_1_, ...), custom_call_target="tpu_custom_call" | custom-call | flops 3623878656 | bytes 15728640 | tf_op jit(solution)/shard_map/pallas_call | solution.py:183
  117.2 3.3 %collective-permute-start.8 = (bf16[48,2048]{1,0:T(8,128)(2,1)S(1)}, bf16[48,2048]{1,0:T(8,128)(2,1)S(1)}, u32[]{:S(2)}, u32[]{:S(2)}) collective-permute-start(bf16[48,2048]{1,0:T(8,128)(2,1)S(1)} %get-tuple-element.26), channel_id=1, source_target_pairs={{0,3},{1,0},{2,1},{3,2},{4,7},{5,4},{6,5},{7,6},{8,11},{9,8},{10,9... | collective-permute-start | bytes 589832 | tf_op jit(solution)/shard_map/ppermute | solution.py:21
  120.8 3.3 %collective-permute-start.18 = (bf16[96,2048]{1,0:T(8,128)(2,1)S(1)}, bf16[96,2048]{1,0:T(8,128)(2,1)S(1)}, u32[]{:S(2)}, u32[]{:S(2)}) collective-permute-start(bf16[96,2048]{1,0:T(8,128)(2,1)S(1)} %pad_maximum_fusion.3), channel_id=1, source_target_pairs={{0,3},{1,0},{2,1},{3,2},{4,7},{5,4},{6,5},{7,6},{8,11},{9,8},{10,9... | collective-permute-start | bytes 1179656 | tf_op jit(solution)/shard_map/ppermute | solution.py:21
  124.2 5.5 %collective-permute-done.16 = bf16[96,2048]{1,0:T(8,128)(2,1)S(1)} collective-permute-done((bf16[96,2048]{1,0:T(8,128)(2,1)S(1)}, bf16[96,2048]{1,0:T(8,128)(2,1)S(1)}, u32[]{:S(2)}, u32[]{:S(2)}) %collective-permute-start.16) | collective-permute-done | bytes 393248 | tf_op jit(solution)/shard_map/ppermute | solution.py:21
  131.5 1.4 shard_map.88
  132.9 11.5 %all-to-all-start.3 = ((bf16[16,24,512]{2,1,0:T(8,128)(2,1)}), bf16[16,24,512]{2,1,0:T(8,128)(2,1)S(1)}, u32[]{:S(2)}, u32[]{:S(2)}) async-start(bf16[16,24,512]{2,1,0:T(8,128)(2,1)} %bitcast.7), calls=%async_computation.3 | async-start | bytes 786432 | tf_op jit(solution)/shard_map/all_to_all | solution.py:31
  144.5 3.4 %collective-permute-start.9 = (bf16[96,2048]{1,0:T(8,128)(2,1)S(1)}, bf16[96,2048]{1,0:T(8,128)(2,1)S(1)}, u32[]{:S(2)}, u32[]{:S(2)}) collective-permute-start(bf16[96,2048]{1,0:T(8,128)(2,1)S(1)} %pad_maximum_fusion.1), channel_id=1, source_target_pairs={{0,3},{1,0},{2,1},{3,2},{4,7},{5,4},{6,5},{7,6},{8,11},{9,8},{10,9... | collective-permute-start | bytes 1179656 | tf_op jit(solution)/shard_map/ppermute | solution.py:21
  148.0 8.3 %collective-permute-done.9 = bf16[96,2048]{1,0:T(8,128)(2,1)S(1)} collective-permute-done((bf16[96,2048]{1,0:T(8,128)(2,1)S(1)}, bf16[96,2048]{1,0:T(8,128)(2,1)S(1)}, u32[]{:S(2)}, u32[]{:S(2)}) %collective-permute-start.9) | collective-permute-done | bytes 393248 | tf_op jit(solution)/shard_map/ppermute | solution.py:21
  156.7 1.4 collective-permute-done.10.got
  158.1 1.4 shard_map.85
  159.5 9.0 %all-to-all-done.3 = bf16[16,24,512]{2,1,0:T(8,128)(2,1)S(1)} async-done(((bf16[16,24,512]{2,1,0:T(8,128)(2,1)}), bf16[16,24,512]{2,1,0:T(8,128)(2,1)S(1)}, u32[]{:S(2)}, u32[]{:S(2)}) %all-to-all-start.3) | async-done | bytes 393248 | tf_op jit(solution)/shard_map/all_to_all | solution.py:31
  168.5 6.0 %all-to-all-start.1 = ((bf16[16,24,512]{2,1,0:T(8,128)(2,1)}), bf16[16,24,512]{2,1,0:T(8,128)(2,1)S(1)}, u32[]{:S(2)}, u32[]{:S(2)}) async-start(bf16[16,24,512]{2,1,0:T(8,128)(2,1)} %bitcast.3), calls=%async_computation.1 | async-start | bytes 786432 | tf_op jit(solution)/shard_map/all_to_all | solution.py:31
  174.5 3.2 %collective-permute-start.20 = (f32[1,512]{1,0:T(1,128)S(1)}, f32[1,512]{1,0:T(1,128)S(1)}, u32[]{:S(2)}, u32[]{:S(2)}) collective-permute-start(f32[1,512]{1,0:T(1,128)S(1)} %bitcast.16), channel_id=1, source_target_pairs={{0,3},{1,0},{2,1},{3,2},{4,7},{5,4},{6,5},{7,6},{8,11},{9,8},{10,9... | collective-permute-start | bytes 6152 | tf_op jit(solution)/shard_map/ppermute | solution.py:21
  178.1 1.3 collective-permute-start.22
  179.6 3.2 %collective-permute-done.21.refs_9_ = f32[1,512]{1,0:T(1,128)S(1)} collective-permute-done((f32[1,512]{1,0:T(1,128)S(1)}, f32[1,512]{1,0:T(1,128)S(1)}, u32[]{:S(2)}, u32[]{:S(2)}) %collective-permute-start.21) | collective-permute-done | bytes 2080 | tf_op jit(solution)/shard_map/ppermute | solution.py:21
  182.9 15.5 %all-to-all-done.1 = bf16[16,24,512]{2,1,0:T(8,128)(2,1)S(1)} async-done(((bf16[16,24,512]{2,1,0:T(8,128)(2,1)}), bf16[16,24,512]{2,1,0:T(8,128)(2,1)S(1)}, u32[]{:S(2)}, u32[]{:S(2)}) %all-to-all-start.1) | async-done | bytes 393248 | tf_op jit(solution)/shard_map/all_to_all | solution.py:31
  198.4 1.7 shard_map.89
  200.2 3.2 %collective-permute-start.23 = (bf16[64,512]{1,0:T(8,128)(2,1)S(1)}, bf16[64,512]{1,0:T(8,128)(2,1)S(1)}, u32[]{:S(2)}, u32[]{:S(2)}) collective-permute-start(bf16[64,512]{1,0:T(8,128)(2,1)S(1)} %get-tuple-element.33), channel_id=1, source_target_pairs={{0,3},{1,0},{2,1},{3,2},{4,7},{5,4},{6,5},{7,6},{8,11},{9,8},{10,9... | collective-permute-start | bytes 196616 | tf_op jit(solution)/shard_map/ppermute | solution.py:21
  205.3 3.9 %collective-permute-done.24 = bf16[64,512]{1,0:T(8,128)(2,1)S(1)} collective-permute-done((bf16[64,512]{1,0:T(8,128)(2,1)S(1)}, bf16[64,512]{1,0:T(8,128)(2,1)S(1)}, u32[]{:S(2)}, u32[]{:S(2)}) %collective-permute-start.24) | collective-permute-done | bytes 65568 | tf_op jit(solution)/shard_map/ppermute | solution.py:21
  (78 shorter events, 12.6 us)
Async XLA Ops:
  0.0 2.1 %collective-permute-start = (bf16[64,2048]{1,0:T(8,128)(2,1)}, bf16[64,2048]{1,0:T(8,128)(2,1)S(1)}, u32[]{:S(2)}, u32[]{:S(2)}) collective-permute-start(bf16[64,2048]{1,0:T(8,128)(2,1)} %own.1), channel_id=1, source_target_pairs={{0,4},{4,0},{8,12},{12,8},{16,20},{20,16},{24,28},{28,24},{32,36},... | collective-permute-start | bytes 786440 | tf_op jit(solution)/shard_map/ppermute | solution.py:25
  0.9 1.3 collective-permute-start.1
  2.1 1.0 copy-start.1
  53.2 29.9 %all-to-all-start = ((bf16[16,24,512]{2,1,0:T(8,128)(2,1)}), bf16[16,24,512]{2,1,0:T(8,128)(2,1)S(1)}, u32[]{:S(2)}, u32[]{:S(2)}) async-start(bf16[16,24,512]{2,1,0:T(8,128)(2,1)} %bitcast.1), calls=%async_computation | async-start | bytes 786432 | tf_op jit(solution)/shard_map/all_to_all | solution.py:31
  59.7 27.3 %collective-permute-start.12 = (bf16[96,2048]{1,0:T(8,128)(2,1)S(1)}, bf16[96,2048]{1,0:T(8,128)(2,1)S(1)}, u32[]{:S(2)}, u32[]{:S(2)}) collective-permute-start(bf16[96,2048]{1,0:T(8,128)(2,1)S(1)} %shard_map.86.refs_0_), channel_id=1, source_target_pairs={{0,1},{1,2},{2,3},{3,0},{4,5},{5,6},{6,7},{7,4},{8,9},{9,10},{10,1... | collective-permute-start | bytes 1179656 | tf_op jit(solution)/shard_map/ppermute | solution.py:21
  61.5 26.0 %collective-permute-start.11 = (bf16[96,2048]{1,0:T(8,128)(2,1)S(1)}, bf16[96,2048]{1,0:T(8,128)(2,1)S(1)}, u32[]{:S(2)}, u32[]{:S(2)}) collective-permute-start(bf16[96,2048]{1,0:T(8,128)(2,1)S(1)} %shard_map.86.refs_0_), channel_id=1, source_target_pairs={{0,3},{1,0},{2,1},{3,2},{4,7},{5,4},{6,5},{7,6},{8,11},{9,8},{10,9... | collective-permute-start | bytes 1179656 | tf_op jit(solution)/shard_map/ppermute | solution.py:21
  83.6 11.2 %collective-permute-start.3 = (bf16[96,2048]{1,0:T(8,128)(2,1)S(1)}, bf16[96,2048]{1,0:T(8,128)(2,1)S(1)}, u32[]{:S(2)}, u32[]{:S(2)}) collective-permute-start(bf16[96,2048]{1,0:T(8,128)(2,1)S(1)} %shard_map.83.refs_0_), channel_id=1, source_target_pairs={{0,1},{1,2},{2,3},{3,0},{4,5},{5,6},{6,7},{7,4},{8,9},{9,10},{10,1... | collective-permute-start | bytes 1179656 | tf_op jit(solution)/shard_map/ppermute | solution.py:21
  85.3 9.6 %collective-permute-start.2 = (bf16[96,2048]{1,0:T(8,128)(2,1)S(1)}, bf16[96,2048]{1,0:T(8,128)(2,1)S(1)}, u32[]{:S(2)}, u32[]{:S(2)}) collective-permute-start(bf16[96,2048]{1,0:T(8,128)(2,1)S(1)} %shard_map.83.refs_0_), channel_id=1, source_target_pairs={{0,3},{1,0},{2,1},{3,2},{4,7},{5,4},{6,5},{7,6},{8,11},{9,8},{10,9... | collective-permute-start | bytes 1179656 | tf_op jit(solution)/shard_map/ppermute | solution.py:21
  87.0 11.5 %collective-permute-start.13 = (bf16[48,2048]{1,0:T(8,128)(2,1)S(1)}, bf16[48,2048]{1,0:T(8,128)(2,1)S(1)}, u32[]{:S(2)}, u32[]{:S(2)}) collective-permute-start(bf16[48,2048]{1,0:T(8,128)(2,1)S(1)} %slice.102), channel_id=1, source_target_pairs={{0,1},{1,2},{2,3},{3,0},{4,5},{5,6},{6,7},{7,4},{8,9},{9,10},{10,1... | collective-permute-start | bytes 589832 | tf_op jit(solution)/shard_map/ppermute | solution.py:21
  87.5 11.0 %collective-permute-start.14 = (bf16[48,2048]{1,0:T(8,128)(2,1)S(1)}, bf16[48,2048]{1,0:T(8,128)(2,1)S(1)}, u32[]{:S(2)}, u32[]{:S(2)}) collective-permute-start(bf16[48,2048]{1,0:T(8,128)(2,1)S(1)} %slice.103), channel_id=1, source_target_pairs={{0,3},{1,0},{2,1},{3,2},{4,7},{5,4},{6,5},{7,6},{8,11},{9,8},{10,9... | collective-permute-start | bytes 589832 | tf_op jit(solution)/shard_map/ppermute | solution.py:21
  94.8 14.7 %collective-permute-start.4 = (bf16[48,2048]{1,0:T(8,128)(2,1)S(1)}, bf16[48,2048]{1,0:T(8,128)(2,1)S(1)}, u32[]{:S(2)}, u32[]{:S(2)}) collective-permute-start(bf16[48,2048]{1,0:T(8,128)(2,1)S(1)} %slice.96), channel_id=1, source_target_pairs={{0,1},{1,2},{2,3},{3,0},{4,5},{5,6},{6,7},{7,4},{8,9},{9,10},{10,1... | collective-permute-start | bytes 589832 | tf_op jit(solution)/shard_map/ppermute | solution.py:21
  95.0 14.5 %collective-permute-start.5 = (bf16[48,2048]{1,0:T(8,128)(2,1)S(1)}, bf16[48,2048]{1,0:T(8,128)(2,1)S(1)}, u32[]{:S(2)}, u32[]{:S(2)}) collective-permute-start(bf16[48,2048]{1,0:T(8,128)(2,1)S(1)} %slice.97), channel_id=1, source_target_pairs={{0,3},{1,0},{2,1},{3,2},{4,7},{5,4},{6,5},{7,6},{8,11},{9,8},{10,9... | collective-permute-start | bytes 589832 | tf_op jit(solution)/shard_map/ppermute | solution.py:21
  106.0 14.5 %collective-permute-start.15 = (bf16[48,2048]{1,0:T(8,128)(2,1)S(1)}, bf16[48,2048]{1,0:T(8,128)(2,1)S(1)}, u32[]{:S(2)}, u32[]{:S(2)}) collective-permute-start(bf16[48,2048]{1,0:T(8,128)(2,1)S(1)} %get-tuple-element.30), channel_id=1, source_target_pairs={{0,1},{1,2},{2,3},{3,0},{4,5},{5,6},{6,7},{7,4},{8,9},{9,10},{10,1... | collective-permute-start | bytes 589832 | tf_op jit(solution)/shard_map/ppermute | solution.py:21
  106.1 14.6 %collective-permute-start.17 = (bf16[48,2048]{1,0:T(8,128)(2,1)S(1)}, bf16[48,2048]{1,0:T(8,128)(2,1)S(1)}, u32[]{:S(2)}, u32[]{:S(2)}) collective-permute-start(bf16[48,2048]{1,0:T(8,128)(2,1)S(1)} %get-tuple-element.32), channel_id=1, source_target_pairs={{0,3},{1,0},{2,1},{3,2},{4,7},{5,4},{6,5},{7,6},{8,11},{9,8},{10,9... | collective-permute-start | bytes 589832 | tf_op jit(solution)/shard_map/ppermute | solution.py:21
  117.0 7.2 %collective-permute-start.6 = (bf16[48,2048]{1,0:T(8,128)(2,1)S(1)}, bf16[48,2048]{1,0:T(8,128)(2,1)S(1)}, u32[]{:S(2)}, u32[]{:S(2)}) collective-permute-start(bf16[48,2048]{1,0:T(8,128)(2,1)S(1)} %get-tuple-element.24), channel_id=1, source_target_pairs={{0,1},{1,2},{2,3},{3,0},{4,5},{5,6},{6,7},{7,4},{8,9},{9,10},{10,1... | collective-permute-start | bytes 589832 | tf_op jit(solution)/shard_map/ppermute | solution.py:21
  117.2 27.3 %collective-permute-start.8 = (bf16[48,2048]{1,0:T(8,128)(2,1)S(1)}, bf16[48,2048]{1,0:T(8,128)(2,1)S(1)}, u32[]{:S(2)}, u32[]{:S(2)}) collective-permute-start(bf16[48,2048]{1,0:T(8,128)(2,1)S(1)} %get-tuple-element.26), channel_id=1, source_target_pairs={{0,3},{1,0},{2,1},{3,2},{4,7},{5,4},{6,5},{7,6},{8,11},{9,8},{10,9... | collective-permute-start | bytes 589832 | tf_op jit(solution)/shard_map/ppermute | solution.py:21
  120.6 9.1 %collective-permute-start.16 = (bf16[96,2048]{1,0:T(8,128)(2,1)S(1)}, bf16[96,2048]{1,0:T(8,128)(2,1)S(1)}, u32[]{:S(2)}, u32[]{:S(2)}) collective-permute-start(bf16[96,2048]{1,0:T(8,128)(2,1)S(1)} %pad_maximum_fusion.2), channel_id=1, source_target_pairs={{0,1},{1,2},{2,3},{3,0},{4,5},{5,6},{6,7},{7,4},{8,9},{9,10},{10,1... | collective-permute-start | bytes 1179656 | tf_op jit(solution)/shard_map/ppermute | solution.py:21
  120.8 8.9 %collective-permute-start.18 = (bf16[96,2048]{1,0:T(8,128)(2,1)S(1)}, bf16[96,2048]{1,0:T(8,128)(2,1)S(1)}, u32[]{:S(2)}, u32[]{:S(2)}) collective-permute-start(bf16[96,2048]{1,0:T(8,128)(2,1)S(1)} %pad_maximum_fusion.3), channel_id=1, source_target_pairs={{0,3},{1,0},{2,1},{3,2},{4,7},{5,4},{6,5},{7,6},{8,11},{9,8},{10,9... | collective-permute-start | bytes 1179656 | tf_op jit(solution)/shard_map/ppermute | solution.py:21
  130.0 1.6 collective-permute-start.19
  130.2 17.8 %collective-permute-start.7 = (bf16[96,2048]{1,0:T(8,128)(2,1)S(1)}, bf16[96,2048]{1,0:T(8,128)(2,1)S(1)}, u32[]{:S(2)}, u32[]{:S(2)}) collective-permute-start(bf16[96,2048]{1,0:T(8,128)(2,1)S(1)} %pad_maximum_fusion), channel_id=1, source_target_pairs={{0,1},{1,2},{2,3},{3,0},{4,5},{5,6},{6,7},{7,4},{8,9},{9,10},{10,1... | collective-permute-start | bytes 1179656 | tf_op jit(solution)/shard_map/ppermute | solution.py:21
  132.9 35.6 %all-to-all-start.3 = ((bf16[16,24,512]{2,1,0:T(8,128)(2,1)}), bf16[16,24,512]{2,1,0:T(8,128)(2,1)S(1)}, u32[]{:S(2)}, u32[]{:S(2)}) async-start(bf16[16,24,512]{2,1,0:T(8,128)(2,1)} %bitcast.7), calls=%async_computation.3 | async-start | bytes 786432 | tf_op jit(solution)/shard_map/all_to_all | solution.py:31
  144.5 11.8 %collective-permute-start.9 = (bf16[96,2048]{1,0:T(8,128)(2,1)S(1)}, bf16[96,2048]{1,0:T(8,128)(2,1)S(1)}, u32[]{:S(2)}, u32[]{:S(2)}) collective-permute-start(bf16[96,2048]{1,0:T(8,128)(2,1)S(1)} %pad_maximum_fusion.1), channel_id=1, source_target_pairs={{0,3},{1,0},{2,1},{3,2},{4,7},{5,4},{6,5},{7,6},{8,11},{9,8},{10,9... | collective-permute-start | bytes 1179656 | tf_op jit(solution)/shard_map/ppermute | solution.py:21
  148.0 26.5 %copy-start.3 = (f32[512]{0:T(512)S(1)}, f32[512]{0:T(512)}, u32[]{:S(2)}) copy-start(f32[512]{0:T(512)} %param.15) | copy-start | bytes 6148
  148.0 31.4 %copy-start.4 = (f32[256,2]{0,1:T(2,128)S(1)}, f32[256,2]{0,1:T(2,128)}, u32[]{:S(2)}) copy-start(f32[256,2]{0,1:T(2,128)} %param.11) | copy-start | bytes 6148
  156.6 1.6 collective-permute-start.10
  168.5 29.9 %all-to-all-start.1 = ((bf16[16,24,512]{2,1,0:T(8,128)(2,1)}), bf16[16,24,512]{2,1,0:T(8,128)(2,1)S(1)}, u32[]{:S(2)}, u32[]{:S(2)}) async-start(bf16[16,24,512]{2,1,0:T(8,128)(2,1)} %bitcast.3), calls=%async_computation.1 | async-start | bytes 786432 | tf_op jit(solution)/shard_map/all_to_all | solution.py:31
  174.5 5.1 %collective-permute-start.20 = (f32[1,512]{1,0:T(1,128)S(1)}, f32[1,512]{1,0:T(1,128)S(1)}, u32[]{:S(2)}, u32[]{:S(2)}) collective-permute-start(f32[1,512]{1,0:T(1,128)S(1)} %bitcast.16), channel_id=1, source_target_pairs={{0,3},{1,0},{2,1},{3,2},{4,7},{5,4},{6,5},{7,6},{8,11},{9,8},{10,9... | collective-permute-start | bytes 6152 | tf_op jit(solution)/shard_map/ppermute | solution.py:21
  177.7 5.1 %collective-permute-start.21 = (f32[1,512]{1,0:T(1,128)S(1)}, f32[1,512]{1,0:T(1,128)S(1)}, u32[]{:S(2)}, u32[]{:S(2)}) collective-permute-start(f32[1,512]{1,0:T(1,128)S(1)} %bitcast.17), channel_id=1, source_target_pairs={{0,2},{1,3},{2,0},{3,1},{4,6},{5,7},{6,4},{7,5},{8,10},{9,11},{10,... | collective-permute-start | bytes 6152 | tf_op jit(solution)/shard_map/ppermute | solution.py:21
  178.1 4.8 %collective-permute-start.22 = (f32[1,512]{1,0:T(1,128)S(1)}, f32[1,512]{1,0:T(1,128)S(1)}, u32[]{:S(2)}, u32[]{:S(2)}) collective-permute-start(f32[1,512]{1,0:T(1,128)S(1)} %bitcast.18), channel_id=1, source_target_pairs={{0,1},{1,2},{2,3},{3,0},{4,5},{5,6},{6,7},{7,4},{8,9},{9,10},{10,1... | collective-permute-start | bytes 6152 | tf_op jit(solution)/shard_map/ppermute | solution.py:21
  200.2 5.1 %collective-permute-start.23 = (bf16[64,512]{1,0:T(8,128)(2,1)S(1)}, bf16[64,512]{1,0:T(8,128)(2,1)S(1)}, u32[]{:S(2)}, u32[]{:S(2)}) collective-permute-start(bf16[64,512]{1,0:T(8,128)(2,1)S(1)} %get-tuple-element.33), channel_id=1, source_target_pairs={{0,3},{1,0},{2,1},{3,2},{4,7},{5,4},{6,5},{7,6},{8,11},{9,8},{10,9... | collective-permute-start | bytes 196616 | tf_op jit(solution)/shard_map/ppermute | solution.py:21
  203.4 5.8 %collective-permute-start.24 = (bf16[64,512]{1,0:T(8,128)(2,1)S(1)}, bf16[64,512]{1,0:T(8,128)(2,1)S(1)}, u32[]{:S(2)}, u32[]{:S(2)}) collective-permute-start(bf16[64,512]{1,0:T(8,128)(2,1)S(1)} %get-tuple-element.34), channel_id=1, source_target_pairs={{0,2},{1,3},{2,0},{3,1},{4,6},{5,7},{6,4},{7,5},{8,10},{9,11},{10,... | collective-permute-start | bytes 196616 | tf_op jit(solution)/shard_map/ppermute | solution.py:21
  203.8 6.1 %collective-permute-start.25 = (bf16[64,512]{1,0:T(8,128)(2,1)S(1)}, bf16[64,512]{1,0:T(8,128)(2,1)S(1)}, u32[]{:S(2)}, u32[]{:S(2)}) collective-permute-start(bf16[64,512]{1,0:T(8,128)(2,1)S(1)} %get-tuple-element.35), channel_id=1, source_target_pairs={{0,1},{1,2},{2,3},{3,0},{4,5},{5,6},{6,7},{7,4},{8,9},{9,10},{10,1... | collective-permute-start | bytes 196616 | tf_op jit(solution)/shard_map/ppermute | solution.py:21
  (2 other events, 1.4 us)

commit v2 on v1

--- a/solution.py
+++ b/solution.py
@@ -11,6 +11,7 @@
 EPS = 1e-06
 CHUNKS = 2
 TILE = 256
+OUT_TILE = 512
 NARROW = jnp.bfloat16
 WIDE = jnp.float32
 VMEM_LIMIT = 48 * 1024 * 1024
@@ -80,34 +81,35 @@
 
 
 def expert_kernel(*refs):
-    sources, (wg, wu, wd), sinks, (flat, acc) = refs[:5], refs[5:8], refs[8:13], refs[13:]
-    step = pl.program_id(0)
-
-    @pl.when(step == 0)
-    def _():
-        at = 0
-        for source in sources:
-            flat[at : at + source.shape[0], :] = source[...]
-            at += source.shape[0]
-
-    gate = dot(flat[...], wg[0])
-    up = dot(flat[...], wu[0])
-    hidden = (gate / (1.0 + jnp.exp(-gate)) * up).astype(NARROW)
-    down = dot(hidden, wd[0])
-
-    @pl.when(step == 0)
-    def _():
-        acc[...] = down
-
-    @pl.when(step > 0)
-    def _():
-        acc[...] += down
-
-    @pl.when(step == pl.num_programs(0) - 1)
-    def _():
+    sources, weights, sinks = refs[:5], refs[5:8], refs[8:13]
+    flat, hidden, wg, wu, wd, sems = refs[13:]
+    steps = hidden.shape[1] // TILE
+    loads = []
+    for j in range(steps):
+        part = pl.ds(j * TILE, TILE)
+        for n, (source, kept) in enumerate(zip(weights, (wg, wu))):
+            loads.append(
+                pltpu.make_async_copy(source.at[0, :, part], kept.at[j], sems.at[2 * j + n])
+            )
+    loads.append(pltpu.make_async_copy(weights[2].at[0], wd, sems.at[2 * steps]))
+    for load in loads:
+        load.start()
+    at = 0
+    for source in sources:
+        flat[at : at + source.shape[0], :] = source[...]
+        at += source.shape[0]
+    for j in range(steps):
+        loads[2 * j].wait()
+        loads[2 * j + 1].wait()
+        gate = dot(flat[...], wg[j])
+        up = dot(flat[...], wu[j])
+        hidden[:, j * TILE : (j + 1) * TILE] = (gate / (1.0 + jnp.exp(-gate)) * up).astype(NARROW)
+    loads[2 * steps].wait()
+    for j in range(0, flat.shape[1], OUT_TILE):
+        down = dot(hidden[...], wd[:, j : j + OUT_TILE])
         at = 0
         for sink in sinks:
-            sink[...] = acc[at : at + sink.shape[0], :].astype(sink.dtype)
+            sink[:, j : j + OUT_TILE] = down[at : at + sink.shape[0], :].astype(sink.dtype)
             at += sink.shape[0]
 
 
@@ -175,31 +177,30 @@
 
 
 def expert(sources, w_gate, w_up, w_down):
-    _, width = sources[0].shape
+    width = sources[0].shape[1]
     hidden = w_gate.shape[2]
     total = sum(s.shape[0] for s in sources)
     dtypes = [WIDE] + [NARROW] * (len(sources) - 1)
-    fixed = lambda s: pl.BlockSpec(s.shape, lambda j: (0, 0))
+    vmem = pl.BlockSpec(memory_space=pltpu.VMEM)
     return pl.pallas_call(
         expert_kernel,
-        grid=(hidden // TILE,),
         out_shape=[jax.ShapeDtypeStruct(s.shape, d) for s, d in zip(sources, dtypes)],
-        in_specs=[fixed(s) for s in sources]
-        + [
-            pl.BlockSpec((1, width, TILE), lambda j: (0, 0, j)),
-            pl.BlockSpec((1, width, TILE), lambda j: (0, 0, j)),
-            pl.BlockSpec((1, TILE, width), lambda j: (0, j, 0)),
+        in_specs=[vmem] * len(sources) + [pl.BlockSpec(memory_space=pl.ANY)] * 3,
+        out_specs=[vmem] * len(sources),
+        scratch_shapes=[
+            pltpu.VMEM((total, width), NARROW),
+            pltpu.VMEM((total, hidden), NARROW),
+            pltpu.VMEM((hidden // TILE, width, TILE), NARROW),
+            pltpu.VMEM((hidden // TILE, width, TILE), NARROW),
+            pltpu.VMEM((hidden, width), NARROW),
+            pltpu.SemaphoreType.DMA((2 * (hidden // TILE) + 1,)),
         ],
-        out_specs=[fixed(s) for s in sources],
-        scratch_shapes=[pltpu.VMEM((total, width), NARROW), pltpu.VMEM((total, width), WIDE)],
         cost_estimate=pl.CostEstimate(
             flops=6 * total * width * hidden,
             bytes_accessed=6 * width * hidden + 8 * total * width,
             transcendentals=total * hidden,
         ),
-        compiler_params=pltpu.CompilerParams(
-            dimension_semantics=("arbitrary",), vmem_limit_bytes=VMEM_LIMIT
-        ),
+        compiler_params=pltpu.CompilerParams(vmem_limit_bytes=VMEM_LIMIT),
     )(*sources, w_gate, w_up, w_down)
 
 
@@ -207,13 +208,8 @@
     half = own.shape[0] // 2
     before = rotate(own, "tp", 1)
     after = rotate(own, "tp", -1)
-    return [
-        own,
-        after,
-        rotate(before[:half], "tp", 1),
-        rotate(after[half:], "tp", -1),
-        before,
-    ]
+    low, high = before[:half], after[half:]
+    return [own, after, rotate(low, "tp", 1), rotate(high, "tp", -1), before]
 
 
 def scatter_blocks(blocks):
@@ -225,12 +221,14 @@
         [(up[:half].astype(WIDE) + from_before.astype(WIDE)).astype(NARROW), up[half:]], axis=0
     )
     down = jnp.concatenate(
-        [down[:half], (down[half:].astype(WIDE) + from_after.astype(WIDE)).astype(NARROW)], axis=0
-    )
-    up = rotate(up, "tp", 1).astype(WIDE)
-    down = rotate(down, "tp", -1).astype(WIDE)
+        [down[:half], (down[half:].astype(WIDE) + from_after.astype(WIDE)).astype(NARROW)],
+        axis=0,
+    )
+    up = rotate(up, "tp", 1)
+    down = rotate(down, "tp", -1)
     return [
-        (own[p] + up[p] + down[p]).astype(NARROW) for p in (slice(0, half), slice(half, None))
+        (own[p] + up[p].astype(WIDE) + down[p].astype(WIDE)).astype(NARROW)
+        for p in (slice(0, half), slice(half, None))
     ]
 
 

time: 211 us -> 208 us (0.986)
  Pallas kernels: 21.9 us -> 19 us
    pallas_call x2, Pallas kernels: 15 us -> 12 us  [expert(): pl.pallas_call(expert_kernel, out_shape=[jax.ShapeDtypeStruct(s.shape, d)...]
  transfers between devices with their start and end apart: 29 -> 29, of which waited for: 14 -> 13; matrix products, arithmetic and copies ran while one was open for 1% -> 1% of each run, Pallas kernels for 9% -> 8%
where the time goes in v2:
time: 208 us
  waiting for transfers between devices  73.6 us (35%)
  starting transfers between devices  62.2 us (30%)
  blocking collectives  47.9 us (23%)
  Pallas kernels  19 us (9%)
  local copies, waits for them, and re-layouts  2.78 us (1%)
    all_to_all x1, blocking collectives, exchange(): return lax.all_to_all(value, 'ep', 0, 0, tiled=True, axis_index_groups=same)  47.9 us
    all_to_all x3, waiting for transfers between devices, exchange(): return lax.all_to_all(value, 'ep', 0, 0, tiled=True, axis_index_groups=same)  44.4 us
    ppermute x22, starting transfers between devices, rotate(): lax.ppermute(value, axis, [(i, (i + step) % size) for i in range(size)])  38.2 us
    ppermute x22, waiting for transfers between devices, rotate(): lax.ppermute(value, axis, [(i, (i + step) % size) for i in range(size)])  25.9 us
    all_to_all x3, starting transfers between devices, exchange(): return lax.all_to_all(value, 'ep', 0, 0, tiled=True, axis_index_groups=same)  23.6 us
    pallas_call x2, Pallas kernels, expert(): pl.pallas_call(expert_kernel, out_shape=[jax.ShapeDtypeStruct(s.shape, d)...  12 us
    pallas_call x6, Pallas kernels, call(): pl.pallas_call(functools.partial(kernel, **kwargs), out_shape=[whole(o) f...  6.96 us
  transfers between devices with their start and end apart: 29, of which 13 were waited for; matrix products, arithmetic and copies ran while one was open for 1% of the time, Pallas kernels for 8%

profile of v2, /device:TPU:40, one launch (start us, length us, event | category | flops | bytes accessed | tf_op | source)
XLA Modules:
  0.0 207.7 jit_solution(4139138377337242289)
XLA Ops:
  3.8 1.6 shard_map.82
  5.3 47.9 %all_to_all.20 = bf16[16,24,512]{2,1,0:T(8,128)(2,1)S(1)} all-to-all(bf16[16,24,512]{2,1,0:T(8,128)(2,1)S(1)} %bitcast.14), channel_id=1, replica_groups={{0,8,16,24,32,40,48,56,64,72,80,88,96,104,112,120},{4,12,20,28,36,44,52..., dimensions={0} | all-to-all | bytes 786432 | tf_op jit(solution)/shard_map/all_to_all | solution.py:32
  53.2 6.0 %all-to-all-start = ((bf16[16,24,512]{2,1,0:T(8,128)(2,1)}), bf16[16,24,512]{2,1,0:T(8,128)(2,1)S(1)}, u32[]{:S(2)}, u32[]{:S(2)}) async-start(bf16[16,24,512]{2,1,0:T(8,128)(2,1)} %bitcast.1), calls=%async_computation | async-start | bytes 786432 | tf_op jit(solution)/shard_map/all_to_all | solution.py:32
  59.7 1.7 collective-permute-start.12
  61.5 1.7 collective-permute-start.11
  63.2 20.0 %all-to-all-done = bf16[16,24,512]{2,1,0:T(8,128)(2,1)S(1)} async-done(((bf16[16,24,512]{2,1,0:T(8,128)(2,1)}), bf16[16,24,512]{2,1,0:T(8,128)(2,1)S(1)}, u32[]{:S(2)}, u32[]{:S(2)}) %all-to-all-start) | async-done | bytes 393248 | tf_op jit(solution)/shard_map/all_to_all | solution.py:32
  83.6 1.7 collective-permute-start.3
  85.3 1.7 collective-permute-start.2
  87.5 3.0 %collective-permute-start.14 = (bf16[48,2048]{1,0:T(8,128)(2,1)S(1)}, bf16[48,2048]{1,0:T(8,128)(2,1)S(1)}, u32[]{:S(2)}, u32[]{:S(2)}) collective-permute-start(bf16[48,2048]{1,0:T(8,128)(2,1)S(1)} %slice.103), channel_id=1, source_target_pairs={{0,3},{1,0},{2,1},{3,2},{4,7},{5,4},{6,5},{7,6},{8,11},{9,8},{10,9... | collective-permute-start | bytes 589832 | tf_op jit(solution)/shard_map/ppermute | solution.py:22
  90.8 4.1 %collective-permute-done.3.refs_4_ = bf16[96,2048]{1,0:T(8,128)(2,1)S(1)} collective-permute-done((bf16[96,2048]{1,0:T(8,128)(2,1)S(1)}, bf16[96,2048]{1,0:T(8,128)(2,1)S(1)}, u32[]{:S(2)}, u32[]{:S(2)}) %collective-permute-start.3) | collective-permute-done | bytes 393248 | tf_op jit(solution)/shard_map/ppermute | solution.py:22
  95.0 3.5 %collective-permute-start.5 = (bf16[48,2048]{1,0:T(8,128)(2,1)S(1)}, bf16[48,2048]{1,0:T(8,128)(2,1)S(1)}, u32[]{:S(2)}, u32[]{:S(2)}) collective-permute-start(bf16[48,2048]{1,0:T(8,128)(2,1)S(1)} %slice.97), channel_id=1, source_target_pairs={{0,3},{1,0},{2,1},{3,2},{4,7},{5,4},{6,5},{7,6},{8,11},{9,8},{10,9... | collective-permute-start | bytes 589832 | tf_op jit(solution)/shard_map/ppermute | solution.py:22
  98.5 6.0 %shard_map.87 = (f32[96,2048]{1,0:T(8,128)S(1)}, bf16[96,2048]{1,0:T(8,128)(2,1)S(1)}, bf16[48,2048]{1,0:T(8,128)(2,1)S(1)}, bf16[48,2048]{1,0:T(8,128)(2,1)S(1)}, bf16[96,2048]{1,0:T(8,128)(2,1)S(1)}) custom-call(bf16[96,2048]{1,0:T(8,128)(2,1)S(1)} %shard_map.86.refs_0_, bf16[96,2048]{1,0:T(8,128)(2,1)S(1)} %collective-permute-done.11.refs_1_, ...), custom_call_target="tpu_custom_call" | custom-call | flops 3623878656 | bytes 15728640 | tf_op jit(solution)/shard_map/pallas_call | solution.py:185
  104.7 3.3 %collective-permute-start.17 = (bf16[48,2048]{1,0:T(8,128)(2,1)S(1)}, bf16[48,2048]{1,0:T(8,128)(2,1)S(1)}, u32[]{:S(2)}, u32[]{:S(2)}) collective-permute-start(bf16[48,2048]{1,0:T(8,128)(2,1)S(1)} %get-tuple-element.32), channel_id=1, source_target_pairs={{0,3},{1,0},{2,1},{3,2},{4,7},{5,4},{6,5},{7,6},{8,11},{9,8},{10,9... | collective-permute-start | bytes 589832 | tf_op jit(solution)/shard_map/ppermute | solution.py:22
  108.0 6.0 %shard_map.84 = (f32[96,2048]{1,0:T(8,128)S(1)}, bf16[96,2048]{1,0:T(8,128)(2,1)S(1)}, bf16[48,2048]{1,0:T(8,128)(2,1)S(1)}, bf16[48,2048]{1,0:T(8,128)(2,1)S(1)}, bf16[96,2048]{1,0:T(8,128)(2,1)S(1)}) custom-call(bf16[96,2048]{1,0:T(8,128)(2,1)S(1)} %shard_map.83.refs_0_, bf16[96,2048]{1,0:T(8,128)(2,1)S(1)} %collective-permute-done.2.refs_1_, ...), custom_call_target="tpu_custom_call" | custom-call | flops 3623878656 | bytes 15728640 | tf_op jit(solution)/shard_map/pallas_call | solution.py:185
  114.2 3.3 %collective-permute-start.8 = (bf16[48,2048]{1,0:T(8,128)(2,1)S(1)}, bf16[48,2048]{1,0:T(8,128)(2,1)S(1)}, u32[]{:S(2)}, u32[]{:S(2)}) collective-permute-start(bf16[48,2048]{1,0:T(8,128)(2,1)S(1)} %get-tuple-element.26), channel_id=1, source_target_pairs={{0,3},{1,0},{2,1},{3,2},{4,7},{5,4},{6,5},{7,6},{8,11},{9,8},{10,9... | collective-permute-start | bytes 589832 | tf_op jit(solution)/shard_map/ppermute | solution.py:22
  117.9 3.3 %collective-permute-start.18 = (bf16[96,2048]{1,0:T(8,128)(2,1)S(1)}, bf16[96,2048]{1,0:T(8,128)(2,1)S(1)}, u32[]{:S(2)}, u32[]{:S(2)}) collective-permute-start(bf16[96,2048]{1,0:T(8,128)(2,1)S(1)} %pad_maximum_fusion.3), channel_id=1, source_target_pairs={{0,3},{1,0},{2,1},{3,2},{4,7},{5,4},{6,5},{7,6},{8,11},{9,8},{10,9... | collective-permute-start | bytes 1179656 | tf_op jit(solution)/shard_map/ppermute | solution.py:22
  121.3 5.5 %collective-permute-done.16 = bf16[96,2048]{1,0:T(8,128)(2,1)S(1)} collective-permute-done((bf16[96,2048]{1,0:T(8,128)(2,1)S(1)}, bf16[96,2048]{1,0:T(8,128)(2,1)S(1)}, u32[]{:S(2)}, u32[]{:S(2)}) %collective-permute-start.16) | collective-permute-done | bytes 393248 | tf_op jit(solution)/shard_map/ppermute | solution.py:22
  128.5 1.4 shard_map.88
  129.9 11.6 %all-to-all-start.3 = ((bf16[16,24,512]{2,1,0:T(8,128)(2,1)}), bf16[16,24,512]{2,1,0:T(8,128)(2,1)S(1)}, u32[]{:S(2)}, u32[]{:S(2)}) async-start(bf16[16,24,512]{2,1,0:T(8,128)(2,1)} %bitcast.7), calls=%async_computation.3 | async-start | bytes 786432 | tf_op jit(solution)/shard_map/all_to_all | solution.py:32
  141.6 3.3 %collective-permute-start.9 = (bf16[96,2048]{1,0:T(8,128)(2,1)S(1)}, bf16[96,2048]{1,0:T(8,128)(2,1)S(1)}, u32[]{:S(2)}, u32[]{:S(2)}) collective-permute-start(bf16[96,2048]{1,0:T(8,128)(2,1)S(1)} %pad_maximum_fusion.1), channel_id=1, source_target_pairs={{0,3},{1,0},{2,1},{3,2},{4,7},{5,4},{6,5},{7,6},{8,11},{9,8},{10,9... | collective-permute-start | bytes 1179656 | tf_op jit(solution)/shard_map/ppermute | solution.py:22
  144.8 8.4 %collective-permute-done.9 = bf16[96,2048]{1,0:T(8,128)(2,1)S(1)} collective-permute-done((bf16[96,2048]{1,0:T(8,128)(2,1)S(1)}, bf16[96,2048]{1,0:T(8,128)(2,1)S(1)}, u32[]{:S(2)}, u32[]{:S(2)}) %collective-permute-start.9) | collective-permute-done | bytes 393248 | tf_op jit(solution)/shard_map/ppermute | solution.py:22
  153.5 1.4 collective-permute-done.10.got
  155.0 1.4 shard_map.85
  156.3 9.2 %all-to-all-done.3 = bf16[16,24,512]{2,1,0:T(8,128)(2,1)S(1)} async-done(((bf16[16,24,512]{2,1,0:T(8,128)(2,1)}), bf16[16,24,512]{2,1,0:T(8,128)(2,1)S(1)}, u32[]{:S(2)}, u32[]{:S(2)}) %all-to-all-start.3) | async-done | bytes 393248 | tf_op jit(solution)/shard_map/all_to_all | solution.py:32
  165.5 6.0 %all-to-all-start.1 = ((bf16[16,24,512]{2,1,0:T(8,128)(2,1)}), bf16[16,24,512]{2,1,0:T(8,128)(2,1)S(1)}, u32[]{:S(2)}, u32[]{:S(2)}) async-start(bf16[16,24,512]{2,1,0:T(8,128)(2,1)} %bitcast.3), calls=%async_computation.1 | async-start | bytes 786432 | tf_op jit(solution)/shard_map/all_to_all | solution.py:32
  171.6 3.3 %collective-permute-start.20 = (f32[1,512]{1,0:T(1,128)S(1)}, f32[1,512]{1,0:T(1,128)S(1)}, u32[]{:S(2)}, u32[]{:S(2)}) collective-permute-start(f32[1,512]{1,0:T(1,128)S(1)} %bitcast.16), channel_id=1, source_target_pairs={{0,3},{1,0},{2,1},{3,2},{4,7},{5,4},{6,5},{7,6},{8,11},{9,8},{10,9... | collective-permute-start | bytes 6152 | tf_op jit(solution)/shard_map/ppermute | solution.py:22
  175.5 1.3 collective-permute-start.22
  177.0 3.0 %collective-permute-done.21.refs_9_ = f32[1,512]{1,0:T(1,128)S(1)} collective-permute-done((f32[1,512]{1,0:T(1,128)S(1)}, f32[1,512]{1,0:T(1,128)S(1)}, u32[]{:S(2)}, u32[]{:S(2)}) %collective-permute-start.21) | collective-permute-done | bytes 2080 | tf_op jit(solution)/shard_map/ppermute | solution.py:22
  180.3 15.2 %all-to-all-done.1 = bf16[16,24,512]{2,1,0:T(8,128)(2,1)S(1)} async-done(((bf16[16,24,512]{2,1,0:T(8,128)(2,1)}), bf16[16,24,512]{2,1,0:T(8,128)(2,1)S(1)}, u32[]{:S(2)}, u32[]{:S(2)}) %all-to-all-start.1) | async-done | bytes 393248 | tf_op jit(solution)/shard_map/all_to_all | solution.py:32
  195.5 1.7 shard_map.89
  197.2 3.3 %collective-permute-start.23 = (bf16[64,512]{1,0:T(8,128)(2,1)S(1)}, bf16[64,512]{1,0:T(8,128)(2,1)S(1)}, u32[]{:S(2)}, u32[]{:S(2)}) collective-permute-start(bf16[64,512]{1,0:T(8,128)(2,1)S(1)} %get-tuple-element.33), channel_id=1, source_target_pairs={{0,3},{1,0},{2,1},{3,2},{4,7},{5,4},{6,5},{7,6},{8,11},{9,8},{10,9... | collective-permute-start | bytes 196616 | tf_op jit(solution)/shard_map/ppermute | solution.py:22
  202.4 3.9 %collective-permute-done.24 = bf16[64,512]{1,0:T(8,128)(2,1)S(1)} collective-permute-done((bf16[64,512]{1,0:T(8,128)(2,1)S(1)}, bf16[64,512]{1,0:T(8,128)(2,1)S(1)}, u32[]{:S(2)}, u32[]{:S(2)}) %collective-permute-start.24) | collective-permute-done | bytes 65568 | tf_op jit(solution)/shard_map/ppermute | solution.py:22
  (74 shorter events, 12.8 us)
Async XLA Ops:
  0.0 2.1 %collective-permute-start = (bf16[64,2048]{1,0:T(8,128)(2,1)}, bf16[64,2048]{1,0:T(8,128)(2,1)S(1)}, u32[]{:S(2)}, u32[]{:S(2)}) collective-permute-start(bf16[64,2048]{1,0:T(8,128)(2,1)} %own.1), channel_id=1, source_target_pairs={{0,4},{4,0},{8,12},{12,8},{16,20},{20,16},{24,28},{28,24},{32,36},... | collective-permute-start | bytes 786440 | tf_op jit(solution)/shard_map/ppermute | solution.py:26
  0.9 1.3 collective-permute-start.1
  2.1 1.0 copy-start.1
  53.2 29.9 %all-to-all-start = ((bf16[16,24,512]{2,1,0:T(8,128)(2,1)}), bf16[16,24,512]{2,1,0:T(8,128)(2,1)S(1)}, u32[]{:S(2)}, u32[]{:S(2)}) async-start(bf16[16,24,512]{2,1,0:T(8,128)(2,1)} %bitcast.1), calls=%async_computation | async-start | bytes 786432 | tf_op jit(solution)/shard_map/all_to_all | solution.py:32
  59.7 27.3 %collective-permute-start.12 = (bf16[96,2048]{1,0:T(8,128)(2,1)S(1)}, bf16[96,2048]{1,0:T(8,128)(2,1)S(1)}, u32[]{:S(2)}, u32[]{:S(2)}) collective-permute-start(bf16[96,2048]{1,0:T(8,128)(2,1)S(1)} %shard_map.86.refs_0_), channel_id=1, source_target_pairs={{0,1},{1,2},{2,3},{3,0},{4,5},{5,6},{6,7},{7,4},{8,9},{9,10},{10,1... | collective-permute-start | bytes 1179656 | tf_op jit(solution)/shard_map/ppermute | solution.py:22
  61.5 26.0 %collective-permute-start.11 = (bf16[96,2048]{1,0:T(8,128)(2,1)S(1)}, bf16[96,2048]{1,0:T(8,128)(2,1)S(1)}, u32[]{:S(2)}, u32[]{:S(2)}) collective-permute-start(bf16[96,2048]{1,0:T(8,128)(2,1)S(1)} %shard_map.86.refs_0_), channel_id=1, source_target_pairs={{0,3},{1,0},{2,1},{3,2},{4,7},{5,4},{6,5},{7,6},{8,11},{9,8},{10,9... | collective-permute-start | bytes 1179656 | tf_op jit(solution)/shard_map/ppermute | solution.py:22
  83.6 11.2 %collective-permute-start.3 = (bf16[96,2048]{1,0:T(8,128)(2,1)S(1)}, bf16[96,2048]{1,0:T(8,128)(2,1)S(1)}, u32[]{:S(2)}, u32[]{:S(2)}) collective-permute-start(bf16[96,2048]{1,0:T(8,128)(2,1)S(1)} %shard_map.83.refs_0_), channel_id=1, source_target_pairs={{0,1},{1,2},{2,3},{3,0},{4,5},{5,6},{6,7},{7,4},{8,9},{9,10},{10,1... | collective-permute-start | bytes 1179656 | tf_op jit(solution)/shard_map/ppermute | solution.py:22
  85.3 9.6 %collective-permute-start.2 = (bf16[96,2048]{1,0:T(8,128)(2,1)S(1)}, bf16[96,2048]{1,0:T(8,128)(2,1)S(1)}, u32[]{:S(2)}, u32[]{:S(2)}) collective-permute-start(bf16[96,2048]{1,0:T(8,128)(2,1)S(1)} %shard_map.83.refs_0_), channel_id=1, source_target_pairs={{0,3},{1,0},{2,1},{3,2},{4,7},{5,4},{6,5},{7,6},{8,11},{9,8},{10,9... | collective-permute-start | bytes 1179656 | tf_op jit(solution)/shard_map/ppermute | solution.py:22
  87.0 11.5 %collective-permute-start.13 = (bf16[48,2048]{1,0:T(8,128)(2,1)S(1)}, bf16[48,2048]{1,0:T(8,128)(2,1)S(1)}, u32[]{:S(2)}, u32[]{:S(2)}) collective-permute-start(bf16[48,2048]{1,0:T(8,128)(2,1)S(1)} %slice.102), channel_id=1, source_target_pairs={{0,1},{1,2},{2,3},{3,0},{4,5},{5,6},{6,7},{7,4},{8,9},{9,10},{10,1... | collective-permute-start | bytes 589832 | tf_op jit(solution)/shard_map/ppermute | solution.py:22
  87.5 11.0 %collective-permute-start.14 = (bf16[48,2048]{1,0:T(8,128)(2,1)S(1)}, bf16[48,2048]{1,0:T(8,128)(2,1)S(1)}, u32[]{:S(2)}, u32[]{:S(2)}) collective-permute-start(bf16[48,2048]{1,0:T(8,128)(2,1)S(1)} %slice.103), channel_id=1, source_target_pairs={{0,3},{1,0},{2,1},{3,2},{4,7},{5,4},{6,5},{7,6},{8,11},{9,8},{10,9... | collective-permute-start | bytes 589832 | tf_op jit(solution)/shard_map/ppermute | solution.py:22
  94.8 13.2 %collective-permute-start.4 = (bf16[48,2048]{1,0:T(8,128)(2,1)S(1)}, bf16[48,2048]{1,0:T(8,128)(2,1)S(1)}, u32[]{:S(2)}, u32[]{:S(2)}) collective-permute-start(bf16[48,2048]{1,0:T(8,128)(2,1)S(1)} %slice.96), channel_id=1, source_target_pairs={{0,1},{1,2},{2,3},{3,0},{4,5},{5,6},{6,7},{7,4},{8,9},{9,10},{10,1... | collective-permute-start | bytes 589832 | tf_op jit(solution)/shard_map/ppermute | solution.py:22
  95.0 13.0 %collective-permute-start.5 = (bf16[48,2048]{1,0:T(8,128)(2,1)S(1)}, bf16[48,2048]{1,0:T(8,128)(2,1)S(1)}, u32[]{:S(2)}, u32[]{:S(2)}) collective-permute-start(bf16[48,2048]{1,0:T(8,128)(2,1)S(1)} %slice.97), channel_id=1, source_target_pairs={{0,3},{1,0},{2,1},{3,2},{4,7},{5,4},{6,5},{7,6},{8,11},{9,8},{10,9... | collective-permute-start | bytes 589832 | tf_op jit(solution)/shard_map/ppermute | solution.py:22
  104.5 13.0 %collective-permute-start.15 = (bf16[48,2048]{1,0:T(8,128)(2,1)S(1)}, bf16[48,2048]{1,0:T(8,128)(2,1)S(1)}, u32[]{:S(2)}, u32[]{:S(2)}) collective-permute-start(bf16[48,2048]{1,0:T(8,128)(2,1)S(1)} %get-tuple-element.30), channel_id=1, source_target_pairs={{0,1},{1,2},{2,3},{3,0},{4,5},{5,6},{6,7},{7,4},{8,9},{9,10},{10,1... | collective-permute-start | bytes 589832 | tf_op jit(solution)/shard_map/ppermute | solution.py:22
  104.7 13.1 %collective-permute-start.17 = (bf16[48,2048]{1,0:T(8,128)(2,1)S(1)}, bf16[48,2048]{1,0:T(8,128)(2,1)S(1)}, u32[]{:S(2)}, u32[]{:S(2)}) collective-permute-start(bf16[48,2048]{1,0:T(8,128)(2,1)S(1)} %get-tuple-element.32), channel_id=1, source_target_pairs={{0,3},{1,0},{2,1},{3,2},{4,7},{5,4},{6,5},{7,6},{8,11},{9,8},{10,9... | collective-permute-start | bytes 589832 | tf_op jit(solution)/shard_map/ppermute | solution.py:22
  114.1 7.2 %collective-permute-start.6 = (bf16[48,2048]{1,0:T(8,128)(2,1)S(1)}, bf16[48,2048]{1,0:T(8,128)(2,1)S(1)}, u32[]{:S(2)}, u32[]{:S(2)}) collective-permute-start(bf16[48,2048]{1,0:T(8,128)(2,1)S(1)} %get-tuple-element.24), channel_id=1, source_target_pairs={{0,1},{1,2},{2,3},{3,0},{4,5},{5,6},{6,7},{7,4},{8,9},{9,10},{10,1... | collective-permute-start | bytes 589832 | tf_op jit(solution)/shard_map/ppermute | solution.py:22
  114.2 27.3 %collective-permute-start.8 = (bf16[48,2048]{1,0:T(8,128)(2,1)S(1)}, bf16[48,2048]{1,0:T(8,128)(2,1)S(1)}, u32[]{:S(2)}, u32[]{:S(2)}) collective-permute-start(bf16[48,2048]{1,0:T(8,128)(2,1)S(1)} %get-tuple-element.26), channel_id=1, source_target_pairs={{0,3},{1,0},{2,1},{3,2},{4,7},{5,4},{6,5},{7,6},{8,11},{9,8},{10,9... | collective-permute-start | bytes 589832 | tf_op jit(solution)/shard_map/ppermute | solution.py:22
  117.7 9.1 %collective-permute-start.16 = (bf16[96,2048]{1,0:T(8,128)(2,1)S(1)}, bf16[96,2048]{1,0:T(8,128)(2,1)S(1)}, u32[]{:S(2)}, u32[]{:S(2)}) collective-permute-start(bf16[96,2048]{1,0:T(8,128)(2,1)S(1)} %pad_maximum_fusion.2), channel_id=1, source_target_pairs={{0,1},{1,2},{2,3},{3,0},{4,5},{5,6},{6,7},{7,4},{8,9},{9,10},{10,1... | collective-permute-start | bytes 1179656 | tf_op jit(solution)/shard_map/ppermute | solution.py:22
  117.9 8.9 %collective-permute-start.18 = (bf16[96,2048]{1,0:T(8,128)(2,1)S(1)}, bf16[96,2048]{1,0:T(8,128)(2,1)S(1)}, u32[]{:S(2)}, u32[]{:S(2)}) collective-permute-start(bf16[96,2048]{1,0:T(8,128)(2,1)S(1)} %pad_maximum_fusion.3), channel_id=1, source_target_pairs={{0,3},{1,0},{2,1},{3,2},{4,7},{5,4},{6,5},{7,6},{8,11},{9,8},{10,9... | collective-permute-start | bytes 1179656 | tf_op jit(solution)/shard_map/ppermute | solution.py:22
  126.9 1.6 collective-permute-start.19
  127.1 17.8 %collective-permute-start.7 = (bf16[96,2048]{1,0:T(8,128)(2,1)S(1)}, bf16[96,2048]{1,0:T(8,128)(2,1)S(1)}, u32[]{:S(2)}, u32[]{:S(2)}) collective-permute-start(bf16[96,2048]{1,0:T(8,128)(2,1)S(1)} %pad_maximum_fusion), channel_id=1, source_target_pairs={{0,1},{1,2},{2,3},{3,0},{4,5},{5,6},{6,7},{7,4},{8,9},{9,10},{10,1... | collective-permute-start | bytes 1179656 | tf_op jit(solution)/shard_map/ppermute | solution.py:22
  129.9 41.7 %copy-start.3 = (f32[512]{0:T(512)S(1)}, f32[512]{0:T(512)}, u32[]{:S(2)}) copy-start(f32[512]{0:T(512)} %param.15) | copy-start | bytes 6148
  129.9 46.9 %copy-start.4 = (f32[256,2]{0,1:T(2,128)S(1)}, f32[256,2]{0,1:T(2,128)}, u32[]{:S(2)}) copy-start(f32[256,2]{0,1:T(2,128)} %param.11) | copy-start | bytes 6148
  129.9 35.7 %all-to-all-start.3 = ((bf16[16,24,512]{2,1,0:T(8,128)(2,1)}), bf16[16,24,512]{2,1,0:T(8,128)(2,1)S(1)}, u32[]{:S(2)}, u32[]{:S(2)}) async-start(bf16[16,24,512]{2,1,0:T(8,128)(2,1)} %bitcast.7), calls=%async_computation.3 | async-start | bytes 786432 | tf_op jit(solution)/shard_map/all_to_all | solution.py:32
  141.6 11.7 %collective-permute-start.9 = (bf16[96,2048]{1,0:T(8,128)(2,1)S(1)}, bf16[96,2048]{1,0:T(8,128)(2,1)S(1)}, u32[]{:S(2)}, u32[]{:S(2)}) collective-permute-start(bf16[96,2048]{1,0:T(8,128)(2,1)S(1)} %pad_maximum_fusion.1), channel_id=1, source_target_pairs={{0,3},{1,0},{2,1},{3,2},{4,7},{5,4},{6,5},{7,6},{8,11},{9,8},{10,9... | collective-permute-start | bytes 1179656 | tf_op jit(solution)/shard_map/ppermute | solution.py:22
  153.4 1.6 collective-permute-start.10
  165.5 29.9 %all-to-all-start.1 = ((bf16[16,24,512]{2,1,0:T(8,128)(2,1)}), bf16[16,24,512]{2,1,0:T(8,128)(2,1)S(1)}, u32[]{:S(2)}, u32[]{:S(2)}) async-start(bf16[16,24,512]{2,1,0:T(8,128)(2,1)} %bitcast.3), calls=%async_computation.1 | async-start | bytes 786432 | tf_op jit(solution)/shard_map/all_to_all | solution.py:32
  171.6 5.4 %collective-permute-start.20 = (f32[1,512]{1,0:T(1,128)S(1)}, f32[1,512]{1,0:T(1,128)S(1)}, u32[]{:S(2)}, u32[]{:S(2)}) collective-permute-start(f32[1,512]{1,0:T(1,128)S(1)} %bitcast.16), channel_id=1, source_target_pairs={{0,3},{1,0},{2,1},{3,2},{4,7},{5,4},{6,5},{7,6},{8,11},{9,8},{10,9... | collective-permute-start | bytes 6152 | tf_op jit(solution)/shard_map/ppermute | solution.py:22
  174.8 5.1 %collective-permute-start.21 = (f32[1,512]{1,0:T(1,128)S(1)}, f32[1,512]{1,0:T(1,128)S(1)}, u32[]{:S(2)}, u32[]{:S(2)}) collective-permute-start(f32[1,512]{1,0:T(1,128)S(1)} %bitcast.17), channel_id=1, source_target_pairs={{0,2},{1,3},{2,0},{3,1},{4,6},{5,7},{6,4},{7,5},{8,10},{9,11},{10,... | collective-permute-start | bytes 6152 | tf_op jit(solution)/shard_map/ppermute | solution.py:22
  175.5 4.8 %collective-permute-start.22 = (f32[1,512]{1,0:T(1,128)S(1)}, f32[1,512]{1,0:T(1,128)S(1)}, u32[]{:S(2)}, u32[]{:S(2)}) collective-permute-start(f32[1,512]{1,0:T(1,128)S(1)} %bitcast.18), channel_id=1, source_target_pairs={{0,1},{1,2},{2,3},{3,0},{4,5},{5,6},{6,7},{7,4},{8,9},{9,10},{10,1... | collective-permute-start | bytes 6152 | tf_op jit(solution)/shard_map/ppermute | solution.py:22
  197.2 5.2 %collective-permute-start.23 = (bf16[64,512]{1,0:T(8,128)(2,1)S(1)}, bf16[64,512]{1,0:T(8,128)(2,1)S(1)}, u32[]{:S(2)}, u32[]{:S(2)}) collective-permute-start(bf16[64,512]{1,0:T(8,128)(2,1)S(1)} %get-tuple-element.33), channel_id=1, source_target_pairs={{0,3},{1,0},{2,1},{3,2},{4,7},{5,4},{6,5},{7,6},{8,11},{9,8},{10,9... | collective-permute-start | bytes 196616 | tf_op jit(solution)/shard_map/ppermute | solution.py:22
  200.5 5.8 %collective-permute-start.24 = (bf16[64,512]{1,0:T(8,128)(2,1)S(1)}, bf16[64,512]{1,0:T(8,128)(2,1)S(1)}, u32[]{:S(2)}, u32[]{:S(2)}) collective-permute-start(bf16[64,512]{1,0:T(8,128)(2,1)S(1)} %get-tuple-element.34), channel_id=1, source_target_pairs={{0,2},{1,3},{2,0},{3,1},{4,6},{5,7},{6,4},{7,5},{8,10},{9,11},{10,... | collective-permute-start | bytes 196616 | tf_op jit(solution)/shard_map/ppermute | solution.py:22
  201.1 5.8 %collective-permute-start.25 = (bf16[64,512]{1,0:T(8,128)(2,1)S(1)}, bf16[64,512]{1,0:T(8,128)(2,1)S(1)}, u32[]{:S(2)}, u32[]{:S(2)}) collective-permute-start(bf16[64,512]{1,0:T(8,128)(2,1)S(1)} %get-tuple-element.35), channel_id=1, source_target_pairs={{0,1},{1,2},{2,3},{3,0},{4,5},{5,6},{6,7},{7,4},{8,9},{9,10},{10,1... | collective-permute-start | bytes 196616 | tf_op jit(solution)/shard_map/ppermute | solution.py:22
  (2 other events, 1.4 us)

commit v3 on v2

--- a/solution.py
+++ b/solution.py
@@ -81,8 +81,8 @@
 
 
 def expert_kernel(*refs):
-    sources, weights, sinks = refs[:5], refs[5:8], refs[8:13]
-    flat, hidden, wg, wu, wd, sems = refs[13:]
+    flat, hidden, wg, wu, wd, sems = refs[-6:]
+    sinks, weights, sources = refs[-13:-6], refs[-16:-13], refs[:-16]
     steps = hidden.shape[1] // TILE
     loads = []
     for j in range(steps):
@@ -105,12 +105,17 @@
         up = dot(flat[...], wu[j])
         hidden[:, j * TILE : (j + 1) * TILE] = (gate / (1.0 + jnp.exp(-gate)) * up).astype(NARROW)
     loads[2 * steps].wait()
-    for j in range(0, flat.shape[1], OUT_TILE):
-        down = dot(hidden[...], wd[:, j : j + OUT_TILE])
+
+    def column(j, carry):
+        lanes = pl.ds(pl.multiple_of(j * OUT_TILE, OUT_TILE), OUT_TILE)
+        down = dot(hidden[...], wd[:, lanes])
         at = 0
         for sink in sinks:
-            sink[:, j : j + OUT_TILE] = down[at : at + sink.shape[0], :].astype(sink.dtype)
+            sink[:, lanes] = down[at : at + sink.shape[0], :].astype(sink.dtype)
             at += sink.shape[0]
+        return carry
+
+    lax.fori_loop(0, flat.shape[1] // OUT_TILE, column, 0)
 
 
 def leave_kernel(kept, got, back, out, *, groups):
@@ -180,13 +185,15 @@
     width = sources[0].shape[1]
     hidden = w_gate.shape[2]
     total = sum(s.shape[0] for s in sources)
-    dtypes = [WIDE] + [NARROW] * (len(sources) - 1)
+    block = sources[0].shape[0]
+    outs = [jax.ShapeDtypeStruct((block, width), WIDE)]
+    outs += [jax.ShapeDtypeStruct((block // 2, width), NARROW)] * 6
     vmem = pl.BlockSpec(memory_space=pltpu.VMEM)
     return pl.pallas_call(
         expert_kernel,
-        out_shape=[jax.ShapeDtypeStruct(s.shape, d) for s, d in zip(sources, dtypes)],
+        out_shape=outs,
         in_specs=[vmem] * len(sources) + [pl.BlockSpec(memory_space=pl.ANY)] * 3,
-        out_specs=[vmem] * len(sources),
+        out_specs=[vmem] * len(outs),
         scratch_shapes=[
             pltpu.VMEM((total, width), NARROW),
             pltpu.VMEM((total, hidden), NARROW),
@@ -213,22 +220,23 @@
 
 
 def scatter_blocks(blocks):
-    own, up, far_low, far_high, down = blocks
+    own, up_low, up_high, far_low, far_high, down_low, down_high = blocks
     half = own.shape[0] // 2
+
+    def add(a, b):
+        return (a.astype(WIDE) + b.astype(WIDE)).astype(NARROW)
+
     from_before = rotate(far_low, "tp", 1)
     from_after = rotate(far_high, "tp", -1)
-    up = jnp.concatenate(
-        [(up[:half].astype(WIDE) + from_before.astype(WIDE)).astype(NARROW), up[half:]], axis=0
-    )
-    down = jnp.concatenate(
-        [down[:half], (down[half:].astype(WIDE) + from_after.astype(WIDE)).astype(NARROW)],
-        axis=0,
-    )
-    up = rotate(up, "tp", 1)
-    down = rotate(down, "tp", -1)
+    up_high = rotate(up_high, "tp", 1)
+    down_low = rotate(down_low, "tp", -1)
+    up_low = add(up_low, from_before)
+    down_high = add(down_high, from_after)
+    up_low = rotate(up_low, "tp", 1)
+    down_high = rotate(down_high, "tp", -1)
     return [
-        (own[p] + up[p].astype(WIDE) + down[p].astype(WIDE)).astype(NARROW)
-        for p in (slice(0, half), slice(half, None))
+        (own[:half] + up_low.astype(WIDE) + down_low.astype(WIDE)).astype(NARROW),
+        (own[half:] + up_high.astype(WIDE) + down_high.astype(WIDE)).astype(NARROW),
     ]
 
 
@@ -330,7 +338,10 @@
         flops=4 * CHUNKS * rows * groups * count * lanes,
         moved=4 * rows * lanes,
     )
-    final = [final[0]] + [rotate(final[step], "tp", step) for step in range(1, groups)]
+    kept = [final[0]]
+    for step in range(1, groups):
+        kept.append(rotate(final[step], "tp", step))
+    final = kept
     out = []
     for j in range(groups):
         piece = final[0]

time: 208 us -> 201 us (0.966)
  waiting for transfers between devices: 73.6 us -> 66.2 us
    all_to_all x3, waiting for transfers between devices: 44.4 us -> 23.7 us  [exchange(): return lax.all_to_all(value, 'ep', 0, 0, tiled=True, axis_index_groups=same)]
    ppermute x22 -> x26, waiting for transfers between devices: 25.9 us -> 40.1 us  [rotate(): lax.ppermute(value, axis, [(i, (i + step) % size) for i in range(size)])]
    ppermute x22 -> x26, starting transfers between devices: 38.2 us -> 37.2 us  [rotate(): lax.ppermute(value, axis, [(i, (i + step) % size) for i in range(size)])]
  transfers between devices with their start and end apart: 29 -> 33, of which waited for: 13 -> 16; matrix products, arithmetic and copies ran while one was open for 1% -> 1% of each run, Pallas kernels for 8% -> 8%
where the time goes in v3:
time: 201 us
  waiting for transfers between devices  66.2 us (33%)
  starting transfers between devices  62.1 us (31%)
  blocking collectives  47.9 us (24%)
  Pallas kernels  20.1 us (10%)
  local copies, waits for them, and re-layouts  2.72 us (1%)
    all_to_all x1, blocking collectives, exchange(): return lax.all_to_all(value, 'ep', 0, 0, tiled=True, axis_index_groups=same)  47.9 us
    ppermute x26, waiting for transfers between devices, rotate(): lax.ppermute(value, axis, [(i, (i + step) % size) for i in range(size)])  40.1 us
    ppermute x26, starting transfers between devices, rotate(): lax.ppermute(value, axis, [(i, (i + step) % size) for i in range(size)])  37.2 us
    all_to_all x3, starting transfers between devices, exchange(): return lax.all_to_all(value, 'ep', 0, 0, tiled=True, axis_index_groups=same)  24.5 us
    all_to_all x3, waiting for transfers between devices, exchange(): return lax.all_to_all(value, 'ep', 0, 0, tiled=True, axis_index_groups=same)  23.7 us
    pallas_call x2, Pallas kernels, expert(): pl.pallas_call(expert_kernel, out_shape=outs, in_specs=[vmem] * len(sourc...  13.1 us
    pallas_call x6, Pallas kernels, call(): pl.pallas_call(functools.partial(kernel, **kwargs), out_shape=[whole(o) f...  6.99 us
  transfers between devices with their start and end apart: 33, of which 16 were waited for; matrix products, arithmetic and copies ran while one was open for 1% of the time, Pallas kernels for 8%

profile of v3, /device:TPU:40, one launch (start us, length us, event | category | flops | bytes accessed | tf_op | source)
XLA Modules:
  0.0 200.9 jit_solution(17339675785121045808)
XLA Ops:
  3.8 1.6 shard_map.82
  5.3 47.9 %all_to_all.20 = bf16[16,24,512]{2,1,0:T(8,128)(2,1)S(1)} all-to-all(bf16[16,24,512]{2,1,0:T(8,128)(2,1)S(1)} %bitcast.14), channel_id=1, replica_groups={{0,8,16,24,32,40,48,56,64,72,80,88,96,104,112,120},{4,12,20,28,36,44,52..., dimensions={0} | all-to-all | bytes 786432 | tf_op jit(solution)/shard_map/all_to_all | solution.py:32
  53.2 6.0 %all-to-all-start = ((bf16[16,24,512]{2,1,0:T(8,128)(2,1)}), bf16[16,24,512]{2,1,0:T(8,128)(2,1)S(1)}, u32[]{:S(2)}, u32[]{:S(2)}) async-start(bf16[16,24,512]{2,1,0:T(8,128)(2,1)} %bitcast.1), calls=%async_computation | async-start | bytes 786432 | tf_op jit(solution)/shard_map/all_to_all | solution.py:32
  59.8 1.7 collective-permute-start.14
  61.5 1.7 collective-permute-start.13
  63.2 8.9 %collective-permute-done.14.refs_4_ = bf16[96,2048]{1,0:T(8,128)(2,1)S(1)} collective-permute-done((bf16[96,2048]{1,0:T(8,128)(2,1)S(1)}, bf16[96,2048]{1,0:T(8,128)(2,1)S(1)}, u32[]{:S(2)}, u32[]{:S(2)}) %collective-permute-start.14) | collective-permute-done | bytes 393248 | tf_op jit(solution)/shard_map/ppermute | solution.py:22
  72.4 3.2 %collective-permute-start.16 = (bf16[48,2048]{1,0:T(8,128)(2,1)S(1)}, bf16[48,2048]{1,0:T(8,128)(2,1)S(1)}, u32[]{:S(2)}, u32[]{:S(2)}) collective-permute-start(bf16[48,2048]{1,0:T(8,128)(2,1)S(1)} %slice.35), channel_id=1, source_target_pairs={{0,3},{1,0},{2,1},{3,2},{4,7},{5,4},{6,5},{7,6},{8,11},{9,8},{10,9... | collective-permute-start | bytes 589832 | tf_op jit(solution)/shard_map/ppermute | solution.py:22
  75.5 3.7 %collective-permute-done.15.refs_2_ = bf16[48,2048]{1,0:T(8,128)(2,1)S(1)} collective-permute-done((bf16[48,2048]{1,0:T(8,128)(2,1)S(1)}, bf16[48,2048]{1,0:T(8,128)(2,1)S(1)}, u32[]{:S(2)}, u32[]{:S(2)}) %collective-permute-start.15) | collective-permute-done | bytes 196640 | tf_op jit(solution)/shard_map/ppermute | solution.py:22
  79.3 6.5 %shard_map.87 = (f32[96,2048]{1,0:T(8,128)S(1)}, bf16[48,2048]{1,0:T(8,128)(2,1)S(1)}, bf16[48,2048]{1,0:T(8,128)(2,1)S(1)}, bf16[48,2048]{1,0:T(8,128)(2,1)S(1)...) custom-call(bf16[96,2048]{1,0:T(8,128)(2,1)S(1)} %shard_map.86.refs_0_, ...), custom_call_target="tpu_custom_call" | custom-call | flops 3623878656 | bytes 15728640 | tf_op jit(solution)/shard_map/pallas_call | solution.py:192
  88.4 1.9 collective-permute-start.2
  90.3 1.6 collective-permute-start.21
  91.8 1.9 collective-permute-start.19
  95.0 10.3 %collective-permute-done.21 = bf16[48,2048]{1,0:T(8,128)(2,1)S(1)} collective-permute-done((bf16[48,2048]{1,0:T(8,128)(2,1)S(1)}, bf16[48,2048]{1,0:T(8,128)(2,1)S(1)}, u32[]{:S(2)}, u32[]{:S(2)}) %collective-permute-start.21) | collective-permute-done | bytes 196640 | tf_op jit(solution)/shard_map/ppermute | solution.py:22
  105.3 2.0 %collective-permute-start.18 = (bf16[48,2048]{1,0:T(8,128)(2,1)S(1)}, bf16[48,2048]{1,0:T(8,128)(2,1)S(1)}, u32[]{:S(2)}, u32[]{:S(2)}) collective-permute-start(bf16[48,2048]{1,0:T(8,128)(2,1)S(1)} %add_convert_fusion.3), channel_id=1, source_target_pairs={{0,1},{1,2},{2,3},{3,0},{4,5},{5,6},{6,7},{7,4},{8,9},{9,10},{10,1... | collective-permute-start | bytes 589832 | tf_op jit(solution)/shard_map/ppermute | solution.py:22
  109.6 2.5 %collective-permute-start.5 = (bf16[48,2048]{1,0:T(8,128)(2,1)S(1)}, bf16[48,2048]{1,0:T(8,128)(2,1)S(1)}, u32[]{:S(2)}, u32[]{:S(2)}) collective-permute-start(bf16[48,2048]{1,0:T(8,128)(2,1)S(1)} %slice.33), channel_id=1, source_target_pairs={{0,3},{1,0},{2,1},{3,2},{4,7},{5,4},{6,5},{7,6},{8,11},{9,8},{10,9... | collective-permute-start | bytes 589832 | tf_op jit(solution)/shard_map/ppermute | solution.py:22
  113.4 2.3 %collective-permute-done.4.refs_2_ = bf16[48,2048]{1,0:T(8,128)(2,1)S(1)} collective-permute-done((bf16[48,2048]{1,0:T(8,128)(2,1)S(1)}, bf16[48,2048]{1,0:T(8,128)(2,1)S(1)}, u32[]{:S(2)}, u32[]{:S(2)}) %collective-permute-start.4) | collective-permute-done | bytes 196640 | tf_op jit(solution)/shard_map/ppermute | solution.py:22
  115.7 6.5 %shard_map.84 = (f32[96,2048]{1,0:T(8,128)S(1)}, bf16[48,2048]{1,0:T(8,128)(2,1)S(1)}, bf16[48,2048]{1,0:T(8,128)(2,1)S(1)}, bf16[48,2048]{1,0:T(8,128)(2,1)S(1)...) custom-call(bf16[96,2048]{1,0:T(8,128)(2,1)S(1)} %shard_map.83.refs_0_, ...), custom_call_target="tpu_custom_call" | custom-call | flops 3623878656 | bytes 15728640 | tf_op jit(solution)/shard_map/pallas_call | solution.py:192
  122.2 1.6 collective-permute-start.6
  124.1 2.0 %collective-permute-start.10 = (bf16[48,2048]{1,0:T(8,128)(2,1)S(1)}, bf16[48,2048]{1,0:T(8,128)(2,1)S(1)}, u32[]{:S(2)}, u32[]{:S(2)}) collective-permute-start(bf16[48,2048]{1,0:T(8,128)(2,1)S(1)} %get-tuple-element.32), channel_id=1, source_target_pairs={{0,3},{1,0},{2,1},{3,2},{4,7},{5,4},{6,5},{7,6},{8,11},{9,8},{10,9... | collective-permute-start | bytes 589832 | tf_op jit(solution)/shard_map/ppermute | solution.py:22
  126.1 2.0 collective-permute-start.8
  129.5 11.8 %all-to-all-start.3 = ((bf16[16,24,512]{2,1,0:T(8,128)(2,1)}), bf16[16,24,512]{2,1,0:T(8,128)(2,1)S(1)}, u32[]{:S(2)}, u32[]{:S(2)}) async-start(bf16[16,24,512]{2,1,0:T(8,128)(2,1)} %bitcast.7), calls=%async_computation.3 | async-start | bytes 786432 | tf_op jit(solution)/shard_map/all_to_all | solution.py:32
  141.6 3.3 %collective-permute-start.11 = (bf16[48,2048]{1,0:T(8,128)(2,1)S(1)}, bf16[48,2048]{1,0:T(8,128)(2,1)S(1)}, u32[]{:S(2)}, u32[]{:S(2)}) collective-permute-start(bf16[48,2048]{1,0:T(8,128)(2,1)S(1)} %add_convert_fusion.5), channel_id=1, source_target_pairs={{0,3},{1,0},{2,1},{3,2},{4,7},{5,4},{6,5},{7,6},{8,11},{9,8},{10,9... | collective-permute-start | bytes 589832 | tf_op jit(solution)/shard_map/ppermute | solution.py:22
  144.9 3.5 %collective-permute-done.7 = bf16[48,2048]{1,0:T(8,128)(2,1)S(1)} collective-permute-done((bf16[48,2048]{1,0:T(8,128)(2,1)S(1)}, bf16[48,2048]{1,0:T(8,128)(2,1)S(1)}, u32[]{:S(2)}, u32[]{:S(2)}) %collective-permute-start.7) | collective-permute-done | bytes 196640 | tf_op jit(solution)/shard_map/ppermute | solution.py:22
  151.5 9.9 %all-to-all-done.3 = bf16[16,24,512]{2,1,0:T(8,128)(2,1)S(1)} async-done(((bf16[16,24,512]{2,1,0:T(8,128)(2,1)}), bf16[16,24,512]{2,1,0:T(8,128)(2,1)S(1)}, u32[]{:S(2)}, u32[]{:S(2)}) %all-to-all-start.3) | async-done | bytes 393248 | tf_op jit(solution)/shard_map/all_to_all | solution.py:32
  161.4 6.8 %all-to-all-start.1 = ((bf16[16,24,512]{2,1,0:T(8,128)(2,1)}), bf16[16,24,512]{2,1,0:T(8,128)(2,1)S(1)}, u32[]{:S(2)}, u32[]{:S(2)}) async-start(bf16[16,24,512]{2,1,0:T(8,128)(2,1)} %bitcast.3), calls=%async_computation.1 | async-start | bytes 786432 | tf_op jit(solution)/shard_map/all_to_all | solution.py:32
  168.2 2.5 %collective-permute-start.24 = (f32[1,512]{1,0:T(1,128)S(1)}, f32[1,512]{1,0:T(1,128)S(1)}, u32[]{:S(2)}, u32[]{:S(2)}) collective-permute-start(f32[1,512]{1,0:T(1,128)S(1)} %bitcast.16), channel_id=1, source_target_pairs={{0,3},{1,0},{2,1},{3,2},{4,7},{5,4},{6,5},{7,6},{8,11},{9,8},{10,9... | collective-permute-start | bytes 6152 | tf_op jit(solution)/shard_map/ppermute | solution.py:22
  172.1 3.8 %collective-permute-done.25.refs_9_ = f32[1,512]{1,0:T(1,128)S(1)} collective-permute-done((f32[1,512]{1,0:T(1,128)S(1)}, f32[1,512]{1,0:T(1,128)S(1)}, u32[]{:S(2)}, u32[]{:S(2)}) %collective-permute-start.25) | collective-permute-done | bytes 2080 | tf_op jit(solution)/shard_map/ppermute | solution.py:22
  175.8 13.7 %all-to-all-done.1 = bf16[16,24,512]{2,1,0:T(8,128)(2,1)S(1)} async-done(((bf16[16,24,512]{2,1,0:T(8,128)(2,1)}), bf16[16,24,512]{2,1,0:T(8,128)(2,1)S(1)}, u32[]{:S(2)}, u32[]{:S(2)}) %all-to-all-start.1) | async-done | bytes 393248 | tf_op jit(solution)/shard_map/all_to_all | solution.py:32
  189.6 1.7 shard_map.89
  192.8 1.9 collective-permute-start.28
  195.7 2.9 %collective-permute-done.28 = bf16[64,512]{1,0:T(8,128)(2,1)S(1)} collective-permute-done((bf16[64,512]{1,0:T(8,128)(2,1)S(1)}, bf16[64,512]{1,0:T(8,128)(2,1)S(1)}, u32[]{:S(2)}, u32[]{:S(2)}) %collective-permute-start.28) | collective-permute-done | bytes 65568 | tf_op jit(solution)/shard_map/ppermute | solution.py:22
  198.6 1.6 collective-permute-done.29
  (74 shorter events, 21.6 us)
Async XLA Ops:
  0.0 2.1 %collective-permute-start = (bf16[64,2048]{1,0:T(8,128)(2,1)}, bf16[64,2048]{1,0:T(8,128)(2,1)S(1)}, u32[]{:S(2)}, u32[]{:S(2)}) collective-permute-start(bf16[64,2048]{1,0:T(8,128)(2,1)} %own.1), channel_id=1, source_target_pairs={{0,4},{4,0},{8,12},{12,8},{16,20},{20,16},{24,28},{28,24},{32,36},... | collective-permute-start | bytes 786440 | tf_op jit(solution)/shard_map/ppermute | solution.py:26
  53.2 33.2 %all-to-all-start = ((bf16[16,24,512]{2,1,0:T(8,128)(2,1)}), bf16[16,24,512]{2,1,0:T(8,128)(2,1)S(1)}, u32[]{:S(2)}, u32[]{:S(2)}) async-start(bf16[16,24,512]{2,1,0:T(8,128)(2,1)} %bitcast.1), calls=%async_computation | async-start | bytes 786432 | tf_op jit(solution)/shard_map/all_to_all | solution.py:32
  59.8 12.3 %collective-permute-start.14 = (bf16[96,2048]{1,0:T(8,128)(2,1)S(1)}, bf16[96,2048]{1,0:T(8,128)(2,1)S(1)}, u32[]{:S(2)}, u32[]{:S(2)}) collective-permute-start(bf16[96,2048]{1,0:T(8,128)(2,1)S(1)} %shard_map.86.refs_0_), channel_id=1, source_target_pairs={{0,1},{1,2},{2,3},{3,0},{4,5},{5,6},{6,7},{7,4},{8,9},{9,10},{10,1... | collective-permute-start | bytes 1179656 | tf_op jit(solution)/shard_map/ppermute | solution.py:22
  61.5 10.9 %collective-permute-start.13 = (bf16[96,2048]{1,0:T(8,128)(2,1)S(1)}, bf16[96,2048]{1,0:T(8,128)(2,1)S(1)}, u32[]{:S(2)}, u32[]{:S(2)}) collective-permute-start(bf16[96,2048]{1,0:T(8,128)(2,1)S(1)} %shard_map.86.refs_0_), channel_id=1, source_target_pairs={{0,3},{1,0},{2,1},{3,2},{4,7},{5,4},{6,5},{7,6},{8,11},{9,8},{10,9... | collective-permute-start | bytes 1179656 | tf_op jit(solution)/shard_map/ppermute | solution.py:22
  72.1 7.2 %collective-permute-start.15 = (bf16[48,2048]{1,0:T(8,128)(2,1)S(1)}, bf16[48,2048]{1,0:T(8,128)(2,1)S(1)}, u32[]{:S(2)}, u32[]{:S(2)}) collective-permute-start(bf16[48,2048]{1,0:T(8,128)(2,1)S(1)} %slice.34), channel_id=1, source_target_pairs={{0,1},{1,2},{2,3},{3,0},{4,5},{5,6},{6,7},{7,4},{8,9},{9,10},{10,1... | collective-permute-start | bytes 589832 | tf_op jit(solution)/shard_map/ppermute | solution.py:22
  72.4 6.9 %collective-permute-start.16 = (bf16[48,2048]{1,0:T(8,128)(2,1)S(1)}, bf16[48,2048]{1,0:T(8,128)(2,1)S(1)}, u32[]{:S(2)}, u32[]{:S(2)}) collective-permute-start(bf16[48,2048]{1,0:T(8,128)(2,1)S(1)} %slice.35), channel_id=1, source_target_pairs={{0,3},{1,0},{2,1},{3,2},{4,7},{5,4},{6,5},{7,6},{8,11},{9,8},{10,9... | collective-permute-start | bytes 589832 | tf_op jit(solution)/shard_map/ppermute | solution.py:22
  85.8 9.1 %collective-permute-start.17 = (bf16[48,2048]{1,0:T(8,128)(2,1)S(1)}, bf16[48,2048]{1,0:T(8,128)(2,1)S(1)}, u32[]{:S(2)}, u32[]{:S(2)}) collective-permute-start(bf16[48,2048]{1,0:T(8,128)(2,1)S(1)} %get-tuple-element.36), channel_id=1, source_target_pairs={{0,1},{1,2},{2,3},{3,0},{4,5},{5,6},{6,7},{7,4},{8,9},{9,10},{10,1... | collective-permute-start | bytes 589832 | tf_op jit(solution)/shard_map/ppermute | solution.py:22
  86.9 20.4 %collective-permute-start.3 = (bf16[96,2048]{1,0:T(8,128)(2,1)S(1)}, bf16[96,2048]{1,0:T(8,128)(2,1)S(1)}, u32[]{:S(2)}, u32[]{:S(2)}) collective-permute-start(bf16[96,2048]{1,0:T(8,128)(2,1)S(1)} %shard_map.83.refs_0_), channel_id=1, source_target_pairs={{0,1},{1,2},{2,3},{3,0},{4,5},{5,6},{6,7},{7,4},{8,9},{9,10},{10,1... | collective-permute-start | bytes 1179656 | tf_op jit(solution)/shard_map/ppermute | solution.py:22
  88.4 20.3 %collective-permute-start.2 = (bf16[96,2048]{1,0:T(8,128)(2,1)S(1)}, bf16[96,2048]{1,0:T(8,128)(2,1)S(1)}, u32[]{:S(2)}, u32[]{:S(2)}) collective-permute-start(bf16[96,2048]{1,0:T(8,128)(2,1)S(1)} %shard_map.83.refs_0_), channel_id=1, source_target_pairs={{0,3},{1,0},{2,1},{3,2},{4,7},{5,4},{6,5},{7,6},{8,11},{9,8},{10,9... | collective-permute-start | bytes 1179656 | tf_op jit(solution)/shard_map/ppermute | solution.py:22
  90.3 15.0 %collective-permute-start.21 = (bf16[48,2048]{1,0:T(8,128)(2,1)S(1)}, bf16[48,2048]{1,0:T(8,128)(2,1)S(1)}, u32[]{:S(2)}, u32[]{:S(2)}) collective-permute-start(bf16[48,2048]{1,0:T(8,128)(2,1)S(1)} %get-tuple-element.40), channel_id=1, source_target_pairs={{0,3},{1,0},{2,1},{3,2},{4,7},{5,4},{6,5},{7,6},{8,11},{9,8},{10,9... | collective-permute-start | bytes 589832 | tf_op jit(solution)/shard_map/ppermute | solution.py:22
  91.8 17.8 %collective-permute-start.19 = (bf16[48,2048]{1,0:T(8,128)(2,1)S(1)}, bf16[48,2048]{1,0:T(8,128)(2,1)S(1)}, u32[]{:S(2)}, u32[]{:S(2)}) collective-permute-start(bf16[48,2048]{1,0:T(8,128)(2,1)S(1)} %get-tuple-element.37), channel_id=1, source_target_pairs={{0,3},{1,0},{2,1},{3,2},{4,7},{5,4},{6,5},{7,6},{8,11},{9,8},{10,9... | collective-permute-start | bytes 589832 | tf_op jit(solution)/shard_map/ppermute | solution.py:22
  94.9 17.3 %collective-permute-start.20 = (bf16[48,2048]{1,0:T(8,128)(2,1)S(1)}, bf16[48,2048]{1,0:T(8,128)(2,1)S(1)}, u32[]{:S(2)}, u32[]{:S(2)}) collective-permute-start(bf16[48,2048]{1,0:T(8,128)(2,1)S(1)} %get-tuple-element.38), channel_id=1, source_target_pairs={{0,1},{1,2},{2,3},{3,0},{4,5},{5,6},{6,7},{7,4},{8,9},{9,10},{10,1... | collective-permute-start | bytes 589832 | tf_op jit(solution)/shard_map/ppermute | solution.py:22
  105.3 6.9 %collective-permute-start.18 = (bf16[48,2048]{1,0:T(8,128)(2,1)S(1)}, bf16[48,2048]{1,0:T(8,128)(2,1)S(1)}, u32[]{:S(2)}, u32[]{:S(2)}) collective-permute-start(bf16[48,2048]{1,0:T(8,128)(2,1)S(1)} %add_convert_fusion.3), channel_id=1, source_target_pairs={{0,1},{1,2},{2,3},{3,0},{4,5},{5,6},{6,7},{7,4},{8,9},{9,10},{10,1... | collective-permute-start | bytes 589832 | tf_op jit(solution)/shard_map/ppermute | solution.py:22
  107.3 5.8 %collective-permute-start.22 = (bf16[48,2048]{1,0:T(8,128)(2,1)S(1)}, bf16[48,2048]{1,0:T(8,128)(2,1)S(1)}, u32[]{:S(2)}, u32[]{:S(2)}) collective-permute-start(bf16[48,2048]{1,0:T(8,128)(2,1)S(1)} %add_convert_fusion.1), channel_id=1, source_target_pairs={{0,3},{1,0},{2,1},{3,2},{4,7},{5,4},{6,5},{7,6},{8,11},{9,8},{10,9... | collective-permute-start | bytes 589832 | tf_op jit(solution)/shard_map/ppermute | solution.py:22
  108.7 7.0 %collective-permute-start.4 = (bf16[48,2048]{1,0:T(8,128)(2,1)S(1)}, bf16[48,2048]{1,0:T(8,128)(2,1)S(1)}, u32[]{:S(2)}, u32[]{:S(2)}) collective-permute-start(bf16[48,2048]{1,0:T(8,128)(2,1)S(1)} %slice.32), channel_id=1, source_target_pairs={{0,1},{1,2},{2,3},{3,0},{4,5},{5,6},{6,7},{7,4},{8,9},{9,10},{10,1... | collective-permute-start | bytes 589832 | tf_op jit(solution)/shard_map/ppermute | solution.py:22
  109.6 6.0 %collective-permute-start.5 = (bf16[48,2048]{1,0:T(8,128)(2,1)S(1)}, bf16[48,2048]{1,0:T(8,128)(2,1)S(1)}, u32[]{:S(2)}, u32[]{:S(2)}) collective-permute-start(bf16[48,2048]{1,0:T(8,128)(2,1)S(1)} %slice.33), channel_id=1, source_target_pairs={{0,3},{1,0},{2,1},{3,2},{4,7},{5,4},{6,5},{7,6},{8,11},{9,8},{10,9... | collective-permute-start | bytes 589832 | tf_op jit(solution)/shard_map/ppermute | solution.py:22
  113.3 14.8 %collective-permute-start.23 = (bf16[48,2048]{1,0:T(8,128)(2,1)S(1)}, bf16[48,2048]{1,0:T(8,128)(2,1)S(1)}, u32[]{:S(2)}, u32[]{:S(2)}) collective-permute-start(bf16[48,2048]{1,0:T(8,128)(2,1)S(1)} %get-tuple-element.45), channel_id=1, source_target_pairs={{0,4},{4,0},{8,12},{12,8},{16,20},{20,16},{24,28},{28,24},{32,36},... | collective-permute-start | bytes 589832 | tf_op jit(solution)/shard_map/ppermute | solution.py:26
  122.2 19.1 %collective-permute-start.6 = (bf16[48,2048]{1,0:T(8,128)(2,1)S(1)}, bf16[48,2048]{1,0:T(8,128)(2,1)S(1)}, u32[]{:S(2)}, u32[]{:S(2)}) collective-permute-start(bf16[48,2048]{1,0:T(8,128)(2,1)S(1)} %get-tuple-element.28), channel_id=1, source_target_pairs={{0,1},{1,2},{2,3},{3,0},{4,5},{5,6},{6,7},{7,4},{8,9},{9,10},{10,1... | collective-permute-start | bytes 589832 | tf_op jit(solution)/shard_map/ppermute | solution.py:22
  124.1 17.5 %collective-permute-start.10 = (bf16[48,2048]{1,0:T(8,128)(2,1)S(1)}, bf16[48,2048]{1,0:T(8,128)(2,1)S(1)}, u32[]{:S(2)}, u32[]{:S(2)}) collective-permute-start(bf16[48,2048]{1,0:T(8,128)(2,1)S(1)} %get-tuple-element.32), channel_id=1, source_target_pairs={{0,3},{1,0},{2,1},{3,2},{4,7},{5,4},{6,5},{7,6},{8,11},{9,8},{10,9... | collective-permute-start | bytes 589832 | tf_op jit(solution)/shard_map/ppermute | solution.py:22
  126.1 18.8 %collective-permute-start.8 = (bf16[48,2048]{1,0:T(8,128)(2,1)S(1)}, bf16[48,2048]{1,0:T(8,128)(2,1)S(1)}, u32[]{:S(2)}, u32[]{:S(2)}) collective-permute-start(bf16[48,2048]{1,0:T(8,128)(2,1)S(1)} %get-tuple-element.29), channel_id=1, source_target_pairs={{0,3},{1,0},{2,1},{3,2},{4,7},{5,4},{6,5},{7,6},{8,11},{9,8},{10,9... | collective-permute-start | bytes 589832 | tf_op jit(solution)/shard_map/ppermute | solution.py:22
  128.1 16.8 %collective-permute-start.9 = (bf16[48,2048]{1,0:T(8,128)(2,1)S(1)}, bf16[48,2048]{1,0:T(8,128)(2,1)S(1)}, u32[]{:S(2)}, u32[]{:S(2)}) collective-permute-start(bf16[48,2048]{1,0:T(8,128)(2,1)S(1)} %get-tuple-element.30), channel_id=1, source_target_pairs={{0,1},{1,2},{2,3},{3,0},{4,5},{5,6},{6,7},{7,4},{8,9},{9,10},{10,1... | collective-permute-start | bytes 589832 | tf_op jit(solution)/shard_map/ppermute | solution.py:22
  129.5 31.9 %all-to-all-start.3 = ((bf16[16,24,512]{2,1,0:T(8,128)(2,1)}), bf16[16,24,512]{2,1,0:T(8,128)(2,1)S(1)}, u32[]{:S(2)}, u32[]{:S(2)}) async-start(bf16[16,24,512]{2,1,0:T(8,128)(2,1)} %bitcast.7), calls=%async_computation.3 | async-start | bytes 786432 | tf_op jit(solution)/shard_map/all_to_all | solution.py:32
  141.4 7.0 %collective-permute-start.7 = (bf16[48,2048]{1,0:T(8,128)(2,1)S(1)}, bf16[48,2048]{1,0:T(8,128)(2,1)S(1)}, u32[]{:S(2)}, u32[]{:S(2)}) collective-permute-start(bf16[48,2048]{1,0:T(8,128)(2,1)S(1)} %add_convert_fusion.7), channel_id=1, source_target_pairs={{0,1},{1,2},{2,3},{3,0},{4,5},{5,6},{6,7},{7,4},{8,9},{9,10},{10,1... | collective-permute-start | bytes 589832 | tf_op jit(solution)/shard_map/ppermute | solution.py:22
  141.6 6.7 %collective-permute-start.11 = (bf16[48,2048]{1,0:T(8,128)(2,1)S(1)}, bf16[48,2048]{1,0:T(8,128)(2,1)S(1)}, u32[]{:S(2)}, u32[]{:S(2)}) collective-permute-start(bf16[48,2048]{1,0:T(8,128)(2,1)S(1)} %add_convert_fusion.5), channel_id=1, source_target_pairs={{0,3},{1,0},{2,1},{3,2},{4,7},{5,4},{6,5},{7,6},{8,11},{9,8},{10,9... | collective-permute-start | bytes 589832 | tf_op jit(solution)/shard_map/ppermute | solution.py:22
  148.5 1.6 collective-permute-start.12
  161.4 28.2 %all-to-all-start.1 = ((bf16[16,24,512]{2,1,0:T(8,128)(2,1)}), bf16[16,24,512]{2,1,0:T(8,128)(2,1)S(1)}, u32[]{:S(2)}, u32[]{:S(2)}) async-start(bf16[16,24,512]{2,1,0:T(8,128)(2,1)} %bitcast.3), calls=%async_computation.1 | async-start | bytes 786432 | tf_op jit(solution)/shard_map/all_to_all | solution.py:32
  168.2 3.9 %collective-permute-start.24 = (f32[1,512]{1,0:T(1,128)S(1)}, f32[1,512]{1,0:T(1,128)S(1)}, u32[]{:S(2)}, u32[]{:S(2)}) collective-permute-start(f32[1,512]{1,0:T(1,128)S(1)} %bitcast.16), channel_id=1, source_target_pairs={{0,3},{1,0},{2,1},{3,2},{4,7},{5,4},{6,5},{7,6},{8,11},{9,8},{10,9... | collective-permute-start | bytes 6152 | tf_op jit(solution)/shard_map/ppermute | solution.py:22
  170.7 5.1 %collective-permute-start.25 = (f32[1,512]{1,0:T(1,128)S(1)}, f32[1,512]{1,0:T(1,128)S(1)}, u32[]{:S(2)}, u32[]{:S(2)}) collective-permute-start(f32[1,512]{1,0:T(1,128)S(1)} %bitcast.17), channel_id=1, source_target_pairs={{0,2},{1,3},{2,0},{3,1},{4,6},{5,7},{6,4},{7,5},{8,10},{9,11},{10,... | collective-permute-start | bytes 6152 | tf_op jit(solution)/shard_map/ppermute | solution.py:22
  170.7 5.1 %collective-permute-start.26 = (f32[1,512]{1,0:T(1,128)S(1)}, f32[1,512]{1,0:T(1,128)S(1)}, u32[]{:S(2)}, u32[]{:S(2)}) collective-permute-start(f32[1,512]{1,0:T(1,128)S(1)} %bitcast.18), channel_id=1, source_target_pairs={{0,1},{1,2},{2,3},{3,0},{4,5},{5,6},{6,7},{7,4},{8,9},{9,10},{10,1... | collective-permute-start | bytes 6152 | tf_op jit(solution)/shard_map/ppermute | solution.py:22
  191.3 4.4 %collective-permute-start.27 = (bf16[64,512]{1,0:T(8,128)(2,1)S(1)}, bf16[64,512]{1,0:T(8,128)(2,1)S(1)}, u32[]{:S(2)}, u32[]{:S(2)}) collective-permute-start(bf16[64,512]{1,0:T(8,128)(2,1)S(1)} %get-tuple-element.41), channel_id=1, source_target_pairs={{0,3},{1,0},{2,1},{3,2},{4,7},{5,4},{6,5},{7,6},{8,11},{9,8},{10,9... | collective-permute-start | bytes 196616 | tf_op jit(solution)/shard_map/ppermute | solution.py:22
  192.8 5.8 %collective-permute-start.28 = (bf16[64,512]{1,0:T(8,128)(2,1)S(1)}, bf16[64,512]{1,0:T(8,128)(2,1)S(1)}, u32[]{:S(2)}, u32[]{:S(2)}) collective-permute-start(bf16[64,512]{1,0:T(8,128)(2,1)S(1)} %get-tuple-element.42), channel_id=1, source_target_pairs={{0,2},{1,3},{2,0},{3,1},{4,6},{5,7},{6,4},{7,5},{8,10},{9,11},{10,... | collective-permute-start | bytes 196616 | tf_op jit(solution)/shard_map/ppermute | solution.py:22
  194.7 5.5 %collective-permute-start.29 = (bf16[64,512]{1,0:T(8,128)(2,1)S(1)}, bf16[64,512]{1,0:T(8,128)(2,1)S(1)}, u32[]{:S(2)}, u32[]{:S(2)}) collective-permute-start(bf16[64,512]{1,0:T(8,128)(2,1)S(1)} %get-tuple-element.43), channel_id=1, source_target_pairs={{0,1},{1,2},{2,3},{3,0},{4,5},{5,6},{6,7},{7,4},{8,9},{9,10},{10,1... | collective-permute-start | bytes 196616 | tf_op jit(solution)/shard_map/ppermute | solution.py:22
  (6 other events, 87.3 us)

commit v4 on v3

--- a/solution.py
+++ b/solution.py
@@ -11,7 +11,7 @@
 EPS = 1e-06
 CHUNKS = 2
 TILE = 256
-OUT_TILE = 512
+OUT_TILE = 1024
 NARROW = jnp.bfloat16
 WIDE = jnp.float32
 VMEM_LIMIT = 48 * 1024 * 1024
@@ -105,17 +105,13 @@
         up = dot(flat[...], wu[j])
         hidden[:, j * TILE : (j + 1) * TILE] = (gate / (1.0 + jnp.exp(-gate)) * up).astype(NARROW)
     loads[2 * steps].wait()
-
-    def column(j, carry):
-        lanes = pl.ds(pl.multiple_of(j * OUT_TILE, OUT_TILE), OUT_TILE)
+    for j in range(0, flat.shape[1], OUT_TILE):
+        lanes = pl.ds(j, OUT_TILE)
         down = dot(hidden[...], wd[:, lanes])
         at = 0
         for sink in sinks:
             sink[:, lanes] = down[at : at + sink.shape[0], :].astype(sink.dtype)
             at += sink.shape[0]
-        return carry
-
-    lax.fori_loop(0, flat.shape[1] // OUT_TILE, column, 0)
 
 
 def leave_kernel(kept, got, back, out, *, groups):
@@ -133,8 +129,7 @@
 def finish_kernel(*refs, capacity, span, groups):
     returned = refs[:CHUNKS]
     own_routes, other_routes, gates, column_key, quarters = refs[CHUNKS : CHUNKS + 5]
-    gains = refs[CHUNKS + 5 : CHUNKS + 5 + groups]
-    outs = refs[CHUNKS + 5 + groups :]
+    outs = refs[CHUNKS + 5 :]
     column, _ = places(own_routes[...], other_routes[...], capacity, span)
     count, choose = gates.shape
     width = groups * returned[0].shape[1]
@@ -160,7 +155,7 @@
     scale = lax.rsqrt(squares / width + EPS)
     for step in range(groups):
         block = total[step * count : (step + 1) * count, :]
-        outs[step][...] = (block * scale * gains[step][...]).astype(NARROW)
+        outs[step][...] = (block * scale).astype(NARROW)
 
 
 def whole(spec):
@@ -211,8 +206,16 @@
     )(*sources, w_gate, w_up, w_down)
 
 
-def gather_blocks(own):
+def gather_blocks(own, k):
     half = own.shape[0] // 2
+    if k == CHUNKS - 1:
+        low, high = own[:half], own[half:]
+        before_low = rotate(low, "tp", 1)
+        after_high = rotate(high, "tp", -1)
+        before_high = rotate(high, "tp", 1)
+        after_low = rotate(low, "tp", -1)
+        far = [rotate(before_low, "tp", 1), rotate(after_high, "tp", -1)]
+        return [own, after_low, after_high, *far, before_low, before_high]
     before = rotate(own, "tp", 1)
     after = rotate(own, "tp", -1)
     low, high = before[:half], after[half:]
@@ -291,9 +294,6 @@
     arrived = []
     for k in range(CHUNKS):
         arrived.append(exchange(outgoing[k].reshape(chips, -1, lanes)).reshape(rows, lanes))
-    gains = [gain_out[None]]
-    gains += [rotate(gain_out[None], "tp", -step) for step in range(1, groups)]
-
     returned = []
     for k in range(CHUNKS):
         (own,) = call(
@@ -305,7 +305,7 @@
             flops=2 * block * rows * width,
             moved=4 * block * width,
         )
-        sources = gather_blocks(own)
+        sources = gather_blocks(own, k)
         parts = expert(sources, w_gate, w_up, w_down)
         kept, sent = scatter_blocks(parts)
         got = partner(sent)
@@ -330,7 +330,6 @@
         own_gates,
         column_key,
         quarters,
-        *gains,
         smem=(CHUNKS + 4,),
         capacity=capacity,
         span=span,
@@ -348,7 +347,8 @@
         for step in range(1, groups):
             piece = jnp.where((me - step) % groups == j, final[step], piece)
         out.append(piece)
-    return jnp.concatenate(out, axis=0)
+    out = jnp.concatenate(out, axis=0).astype(WIDE)
+    return (out * gain_out).astype(NARROW)
 
 
 def solution(mesh):

time: 201 us -> 197 us (0.980)
  waiting for transfers between devices: 66.2 us -> 61.6 us
    ppermute x26 -> x25, waiting for transfers between devices: 40.1 us -> 30.2 us  [rotate(): lax.ppermute(value, axis, [(i, (i + step) % size) for i in range(size)])]
    all_to_all x3, waiting for transfers between devices: 23.7 us -> 29.1 us  [exchange(): return lax.all_to_all(value, 'ep', 0, 0, tiled=True, axis_index_groups=same)]
    ppermute x26 -> x25, starting transfers between devices: 37.2 us -> 38.2 us  [rotate(): lax.ppermute(value, axis, [(i, (i + step) % size) for i in range(size)])]
  transfers between devices with their start and end apart: 33 -> 32, of which waited for: 16 -> 18; matrix products, arithmetic and copies ran while one was open for 1% -> 1% of each run, Pallas kernels for 8% -> 8%
where the time goes in v4:
time: 197 us
  starting transfers between devices  63.3 us (32%)
  waiting for transfers between devices  61.6 us (31%)
  blocking collectives  47.9 us (24%)
  Pallas kernels  19 us (10%)
  local copies, waits for them, and re-layouts  2.73 us (1%)
    all_to_all x1, blocking collectives, exchange(): return lax.all_to_all(value, 'ep', 0, 0, tiled=True, axis_index_groups=same)  47.9 us
    ppermute x25, starting transfers between devices, rotate(): lax.ppermute(value, axis, [(i, (i + step) % size) for i in range(size)])  38.2 us
    ppermute x25, waiting for transfers between devices, rotate(): lax.ppermute(value, axis, [(i, (i + step) % size) for i in range(size)])  30.2 us
    all_to_all x3, waiting for transfers between devices, exchange(): return lax.all_to_all(value, 'ep', 0, 0, tiled=True, axis_index_groups=same)  29.1 us
    all_to_all x3, starting transfers between devices, exchange(): return lax.all_to_all(value, 'ep', 0, 0, tiled=True, axis_index_groups=same)  24.8 us
    pallas_call x2, Pallas kernels, expert(): pl.pallas_call(expert_kernel, out_shape=outs, in_specs=[vmem] * len(sourc...  12 us
    pallas_call x6, Pallas kernels, call(): pl.pallas_call(functools.partial(kernel, **kwargs), out_shape=[whole(o) f...  6.98 us
  transfers between devices with their start and end apart: 32, of which 18 were waited for; matrix products, arithmetic and copies ran while one was open for 1% of the time, Pallas kernels for 8%

profile of v4, /device:TPU:40, one launch (start us, length us, event | category | flops | bytes accessed | tf_op | source)
XLA Modules:
  0.0 196.6 jit_solution(9115643963980280366)
XLA Ops:
  3.8 1.6 shard_map.82
  5.3 47.9 %all_to_all.20 = bf16[16,24,512]{2,1,0:T(8,128)(2,1)S(1)} all-to-all(bf16[16,24,512]{2,1,0:T(8,128)(2,1)S(1)} %bitcast.13), channel_id=1, replica_groups={{0,8,16,24,32,40,48,56,64,72,80,88,96,104,112,120},{4,12,20,28,36,44,52..., dimensions={0} | all-to-all | bytes 786432 | tf_op jit(solution)/shard_map/all_to_all | solution.py:32
  53.2 6.0 %all-to-all-start = ((bf16[16,24,512]{2,1,0:T(8,128)(2,1)}), bf16[16,24,512]{2,1,0:T(8,128)(2,1)S(1)}, u32[]{:S(2)}, u32[]{:S(2)}) async-start(bf16[16,24,512]{2,1,0:T(8,128)(2,1)} %bitcast.1), calls=%async_computation | async-start | bytes 786432 | tf_op jit(solution)/shard_map/all_to_all | solution.py:32
  59.8 1.7 collective-permute-start.15
  61.5 1.7 collective-permute-start.14
  63.2 1.9 collective-permute-start.13
  65.2 2.7 %collective-permute-done.15.refs_5_ = bf16[48,2048]{1,0:T(8,128)(2,1)S(1)} collective-permute-done((bf16[48,2048]{1,0:T(8,128)(2,1)S(1)}, bf16[48,2048]{1,0:T(8,128)(2,1)S(1)}, u32[]{:S(2)}, u32[]{:S(2)}) %collective-permute-start.15) | collective-permute-done | bytes 196640 | tf_op jit(solution)/shard_map/ppermute | solution.py:22
  69.3 2.9 %collective-permute-start.17 = (bf16[48,2048]{1,0:T(8,128)(2,1)S(1)}, bf16[48,2048]{1,0:T(8,128)(2,1)S(1)}, u32[]{:S(2)}, u32[]{:S(2)}) collective-permute-start(bf16[48,2048]{1,0:T(8,128)(2,1)S(1)} %collective-permute-done.14.refs_2_), channel_id=1, source_target_pairs={{0,3},{1,0},{2,1},{3,2},{4,7},{5,4},{6,5},{7,6},{8,11},{9,8},{10,9... | collective-permute-start | bytes 589832 | tf_op jit(solution)/shard_map/ppermute | solution.py:22
  73.5 2.8 %collective-permute-done.16.refs_3_ = bf16[48,2048]{1,0:T(8,128)(2,1)S(1)} collective-permute-done((bf16[48,2048]{1,0:T(8,128)(2,1)S(1)}, bf16[48,2048]{1,0:T(8,128)(2,1)S(1)}, u32[]{:S(2)}, u32[]{:S(2)}) %collective-permute-start.16) | collective-permute-done | bytes 196640 | tf_op jit(solution)/shard_map/ppermute | solution.py:22
  76.3 6.0 %shard_map.87 = (f32[96,2048]{1,0:T(8,128)S(1)}, bf16[48,2048]{1,0:T(8,128)(2,1)S(1)}, bf16[48,2048]{1,0:T(8,128)(2,1)S(1)}, bf16[48,2048]{1,0:T(8,128)(2,1)S(1)...) custom-call(bf16[96,2048]{1,0:T(8,128)(2,1)S(1)} %shard_map.86.refs_0_, ...), custom_call_target="tpu_custom_call" | custom-call | flops 3623878656 | bytes 15728640 | tf_op jit(solution)/shard_map/pallas_call | solution.py:187
  82.3 1.8 collective-permute-start.19
  84.6 1.4 collective-permute-start.3
  86.0 1.9 collective-permute-start.2
  92.0 10.3 %collective-permute-done.23 = bf16[48,2048]{1,0:T(8,128)(2,1)S(1)} collective-permute-done((bf16[48,2048]{1,0:T(8,128)(2,1)S(1)}, bf16[48,2048]{1,0:T(8,128)(2,1)S(1)}, u32[]{:S(2)}, u32[]{:S(2)}) %collective-permute-start.23) | collective-permute-done | bytes 196640 | tf_op jit(solution)/shard_map/ppermute | solution.py:22
  102.2 1.5 collective-permute-start.20
  103.8 1.9 collective-permute-start.24
  106.5 3.1 %collective-permute-start.5 = (bf16[48,2048]{1,0:T(8,128)(2,1)S(1)}, bf16[48,2048]{1,0:T(8,128)(2,1)S(1)}, u32[]{:S(2)}, u32[]{:S(2)}) collective-permute-start(bf16[48,2048]{1,0:T(8,128)(2,1)S(1)} %slice.33), channel_id=1, source_target_pairs={{0,3},{1,0},{2,1},{3,2},{4,7},{5,4},{6,5},{7,6},{8,11},{9,8},{10,9... | collective-permute-start | bytes 589832 | tf_op jit(solution)/shard_map/ppermute | solution.py:22
  110.1 2.5 %collective-permute-done.4.refs_2_ = bf16[48,2048]{1,0:T(8,128)(2,1)S(1)} collective-permute-done((bf16[48,2048]{1,0:T(8,128)(2,1)S(1)}, bf16[48,2048]{1,0:T(8,128)(2,1)S(1)}, u32[]{:S(2)}, u32[]{:S(2)}) %collective-permute-start.4) | collective-permute-done | bytes 196640 | tf_op jit(solution)/shard_map/ppermute | solution.py:22
  112.8 6.0 %shard_map.84 = (f32[96,2048]{1,0:T(8,128)S(1)}, bf16[48,2048]{1,0:T(8,128)(2,1)S(1)}, bf16[48,2048]{1,0:T(8,128)(2,1)S(1)}, bf16[48,2048]{1,0:T(8,128)(2,1)S(1)...) custom-call(bf16[96,2048]{1,0:T(8,128)(2,1)S(1)} %shard_map.83.refs_0_, ...), custom_call_target="tpu_custom_call" | custom-call | flops 3623878656 | bytes 15728640 | tf_op jit(solution)/shard_map/pallas_call | solution.py:187
  120.2 3.0 %collective-permute-start.10 = (bf16[48,2048]{1,0:T(8,128)(2,1)S(1)}, bf16[48,2048]{1,0:T(8,128)(2,1)S(1)}, u32[]{:S(2)}, u32[]{:S(2)}) collective-permute-start(bf16[48,2048]{1,0:T(8,128)(2,1)S(1)} %get-tuple-element.32), channel_id=1, source_target_pairs={{0,3},{1,0},{2,1},{3,2},{4,7},{5,4},{6,5},{7,6},{8,11},{9,8},{10,9... | collective-permute-start | bytes 589832 | tf_op jit(solution)/shard_map/ppermute | solution.py:22
  123.2 2.0 %collective-permute-start.8 = (bf16[48,2048]{1,0:T(8,128)(2,1)S(1)}, bf16[48,2048]{1,0:T(8,128)(2,1)S(1)}, u32[]{:S(2)}, u32[]{:S(2)}) collective-permute-start(bf16[48,2048]{1,0:T(8,128)(2,1)S(1)} %get-tuple-element.29), channel_id=1, source_target_pairs={{0,3},{1,0},{2,1},{3,2},{4,7},{5,4},{6,5},{7,6},{8,11},{9,8},{10,9... | collective-permute-start | bytes 589832 | tf_op jit(solution)/shard_map/ppermute | solution.py:22
  125.2 1.4 shard_map.88
  126.6 11.8 %all-to-all-start.3 = ((bf16[16,24,512]{2,1,0:T(8,128)(2,1)}), bf16[16,24,512]{2,1,0:T(8,128)(2,1)S(1)}, u32[]{:S(2)}, u32[]{:S(2)}) async-start(bf16[16,24,512]{2,1,0:T(8,128)(2,1)} %bitcast.7), calls=%async_computation.3 | async-start | bytes 786432 | tf_op jit(solution)/shard_map/all_to_all | solution.py:32
  138.7 3.3 %collective-permute-start.11 = (bf16[48,2048]{1,0:T(8,128)(2,1)S(1)}, bf16[48,2048]{1,0:T(8,128)(2,1)S(1)}, u32[]{:S(2)}, u32[]{:S(2)}) collective-permute-start(bf16[48,2048]{1,0:T(8,128)(2,1)S(1)} %add_convert_fusion.5), channel_id=1, source_target_pairs={{0,3},{1,0},{2,1},{3,2},{4,7},{5,4},{6,5},{7,6},{8,11},{9,8},{10,9... | collective-permute-start | bytes 589832 | tf_op jit(solution)/shard_map/ppermute | solution.py:22
  142.0 3.4 %collective-permute-done.7 = bf16[48,2048]{1,0:T(8,128)(2,1)S(1)} collective-permute-done((bf16[48,2048]{1,0:T(8,128)(2,1)S(1)}, bf16[48,2048]{1,0:T(8,128)(2,1)S(1)}, u32[]{:S(2)}, u32[]{:S(2)}) %collective-permute-start.7) | collective-permute-done | bytes 196640 | tf_op jit(solution)/shard_map/ppermute | solution.py:22
  145.7 1.4 collective-permute-done.12.got
  148.5 9.0 %all-to-all-done.3 = bf16[16,24,512]{2,1,0:T(8,128)(2,1)S(1)} async-done(((bf16[16,24,512]{2,1,0:T(8,128)(2,1)}), bf16[16,24,512]{2,1,0:T(8,128)(2,1)S(1)}, u32[]{:S(2)}, u32[]{:S(2)}) %all-to-all-start.3) | async-done | bytes 393248 | tf_op jit(solution)/shard_map/all_to_all | solution.py:32
  157.5 7.0 %all-to-all-start.1 = ((bf16[16,24,512]{2,1,0:T(8,128)(2,1)}), bf16[16,24,512]{2,1,0:T(8,128)(2,1)S(1)}, u32[]{:S(2)}, u32[]{:S(2)}) async-start(bf16[16,24,512]{2,1,0:T(8,128)(2,1)} %bitcast.3), calls=%async_computation.1 | async-start | bytes 786432 | tf_op jit(solution)/shard_map/all_to_all | solution.py:32
  164.7 20.1 %all-to-all-done.1 = bf16[16,24,512]{2,1,0:T(8,128)(2,1)S(1)} async-done(((bf16[16,24,512]{2,1,0:T(8,128)(2,1)}), bf16[16,24,512]{2,1,0:T(8,128)(2,1)S(1)}, u32[]{:S(2)}, u32[]{:S(2)}) %all-to-all-start.1) | async-done | bytes 393248 | tf_op jit(solution)/shard_map/all_to_all | solution.py:32
  184.9 1.7 shard_map.89
  186.6 3.0 %collective-permute-start.26 = (bf16[64,512]{1,0:T(8,128)(2,1)S(1)}, bf16[64,512]{1,0:T(8,128)(2,1)S(1)}, u32[]{:S(2)}, u32[]{:S(2)}) collective-permute-start(bf16[64,512]{1,0:T(8,128)(2,1)S(1)} %get-tuple-element.41), channel_id=1, source_target_pairs={{0,3},{1,0},{2,1},{3,2},{4,7},{5,4},{6,5},{7,6},{8,11},{9,8},{10,9... | collective-permute-start | bytes 196616 | tf_op jit(solution)/shard_map/ppermute | solution.py:22
  191.5 4.0 %collective-permute-done.27 = bf16[64,512]{1,0:T(8,128)(2,1)S(1)} collective-permute-done((bf16[64,512]{1,0:T(8,128)(2,1)S(1)}, bf16[64,512]{1,0:T(8,128)(2,1)S(1)}, u32[]{:S(2)}, u32[]{:S(2)}) %collective-permute-start.27) | collective-permute-done | bytes 65568 | tf_op jit(solution)/shard_map/ppermute | solution.py:22
  (71 shorter events, 19.7 us)
Async XLA Ops:
  0.0 2.1 %collective-permute-start = (bf16[64,2048]{1,0:T(8,128)(2,1)}, bf16[64,2048]{1,0:T(8,128)(2,1)S(1)}, u32[]{:S(2)}, u32[]{:S(2)}) collective-permute-start(bf16[64,2048]{1,0:T(8,128)(2,1)} %own.1), channel_id=1, source_target_pairs={{0,4},{4,0},{8,12},{12,8},{16,20},{20,16},{24,28},{28,24},{32,36},... | collective-permute-start | bytes 786440 | tf_op jit(solution)/shard_map/ppermute | solution.py:26
  0.9 1.3 collective-permute-start.1
  53.2 30.9 %all-to-all-start = ((bf16[16,24,512]{2,1,0:T(8,128)(2,1)}), bf16[16,24,512]{2,1,0:T(8,128)(2,1)S(1)}, u32[]{:S(2)}, u32[]{:S(2)}) async-start(bf16[16,24,512]{2,1,0:T(8,128)(2,1)} %bitcast.1), calls=%async_computation | async-start | bytes 786432 | tf_op jit(solution)/shard_map/all_to_all | solution.py:32
  59.8 8.2 %collective-permute-start.15 = (bf16[48,2048]{1,0:T(8,128)(2,1)S(1)}, bf16[48,2048]{1,0:T(8,128)(2,1)S(1)}, u32[]{:S(2)}, u32[]{:S(2)}) collective-permute-start(bf16[48,2048]{1,0:T(8,128)(2,1)S(1)} %get-tuple-element.50), channel_id=1, source_target_pairs={{0,1},{1,2},{2,3},{3,0},{4,5},{5,6},{6,7},{7,4},{8,9},{9,10},{10,1... | collective-permute-start | bytes 589832 | tf_op jit(solution)/shard_map/ppermute | solution.py:22
  61.5 7.8 %collective-permute-start.14 = (bf16[48,2048]{1,0:T(8,128)(2,1)S(1)}, bf16[48,2048]{1,0:T(8,128)(2,1)S(1)}, u32[]{:S(2)}, u32[]{:S(2)}) collective-permute-start(bf16[48,2048]{1,0:T(8,128)(2,1)S(1)} %get-tuple-element.49), channel_id=1, source_target_pairs={{0,3},{1,0},{2,1},{3,2},{4,7},{5,4},{6,5},{7,6},{8,11},{9,8},{10,9... | collective-permute-start | bytes 589832 | tf_op jit(solution)/shard_map/ppermute | solution.py:22
  63.2 10.3 %collective-permute-start.13 = (bf16[48,2048]{1,0:T(8,128)(2,1)S(1)}, bf16[48,2048]{1,0:T(8,128)(2,1)S(1)}, u32[]{:S(2)}, u32[]{:S(2)}) collective-permute-start(bf16[48,2048]{1,0:T(8,128)(2,1)S(1)} %get-tuple-element.50), channel_id=1, source_target_pairs={{0,3},{1,0},{2,1},{3,2},{4,7},{5,4},{6,5},{7,6},{8,11},{9,8},{10,9... | collective-permute-start | bytes 589832 | tf_op jit(solution)/shard_map/ppermute | solution.py:22
  65.1 8.4 %collective-permute-start.18 = (bf16[48,2048]{1,0:T(8,128)(2,1)S(1)}, bf16[48,2048]{1,0:T(8,128)(2,1)S(1)}, u32[]{:S(2)}, u32[]{:S(2)}) collective-permute-start(bf16[48,2048]{1,0:T(8,128)(2,1)S(1)} %get-tuple-element.49), channel_id=1, source_target_pairs={{0,1},{1,2},{2,3},{3,0},{4,5},{5,6},{6,7},{7,4},{8,9},{9,10},{10,1... | collective-permute-start | bytes 589832 | tf_op jit(solution)/shard_map/ppermute | solution.py:22
  67.9 8.3 %collective-permute-start.16 = (bf16[48,2048]{1,0:T(8,128)(2,1)S(1)}, bf16[48,2048]{1,0:T(8,128)(2,1)S(1)}, u32[]{:S(2)}, u32[]{:S(2)}) collective-permute-start(bf16[48,2048]{1,0:T(8,128)(2,1)S(1)} %collective-permute-done.15.refs_5_), channel_id=1, source_target_pairs={{0,1},{1,2},{2,3},{3,0},{4,5},{5,6},{6,7},{7,4},{8,9},{9,10},{10,1... | collective-permute-start | bytes 589832 | tf_op jit(solution)/shard_map/ppermute | solution.py:22
  69.3 7.0 %collective-permute-start.17 = (bf16[48,2048]{1,0:T(8,128)(2,1)S(1)}, bf16[48,2048]{1,0:T(8,128)(2,1)S(1)}, u32[]{:S(2)}, u32[]{:S(2)}) collective-permute-start(bf16[48,2048]{1,0:T(8,128)(2,1)S(1)} %collective-permute-done.14.refs_2_), channel_id=1, source_target_pairs={{0,3},{1,0},{2,1},{3,2},{4,7},{5,4},{6,5},{7,6},{8,11},{9,8},{10,9... | collective-permute-start | bytes 589832 | tf_op jit(solution)/shard_map/ppermute | solution.py:22
  82.3 9.3 %collective-permute-start.19 = (bf16[48,2048]{1,0:T(8,128)(2,1)S(1)}, bf16[48,2048]{1,0:T(8,128)(2,1)S(1)}, u32[]{:S(2)}, u32[]{:S(2)}) collective-permute-start(bf16[48,2048]{1,0:T(8,128)(2,1)S(1)} %get-tuple-element.36), channel_id=1, source_target_pairs={{0,1},{1,2},{2,3},{3,0},{4,5},{5,6},{6,7},{7,4},{8,9},{9,10},{10,1... | collective-permute-start | bytes 589832 | tf_op jit(solution)/shard_map/ppermute | solution.py:22
  84.6 19.2 %collective-permute-start.3 = (bf16[96,2048]{1,0:T(8,128)(2,1)S(1)}, bf16[96,2048]{1,0:T(8,128)(2,1)S(1)}, u32[]{:S(2)}, u32[]{:S(2)}) collective-permute-start(bf16[96,2048]{1,0:T(8,128)(2,1)S(1)} %shard_map.83.refs_0_), channel_id=1, source_target_pairs={{0,1},{1,2},{2,3},{3,0},{4,5},{5,6},{6,7},{7,4},{8,9},{9,10},{10,1... | collective-permute-start | bytes 1179656 | tf_op jit(solution)/shard_map/ppermute | solution.py:22
  86.0 19.6 %collective-permute-start.2 = (bf16[96,2048]{1,0:T(8,128)(2,1)S(1)}, bf16[96,2048]{1,0:T(8,128)(2,1)S(1)}, u32[]{:S(2)}, u32[]{:S(2)}) collective-permute-start(bf16[96,2048]{1,0:T(8,128)(2,1)S(1)} %shard_map.83.refs_0_), channel_id=1, source_target_pairs={{0,3},{1,0},{2,1},{3,2},{4,7},{5,4},{6,5},{7,6},{8,11},{9,8},{10,9... | collective-permute-start | bytes 1179656 | tf_op jit(solution)/shard_map/ppermute | solution.py:22
  87.9 14.3 %collective-permute-start.23 = (bf16[48,2048]{1,0:T(8,128)(2,1)S(1)}, bf16[48,2048]{1,0:T(8,128)(2,1)S(1)}, u32[]{:S(2)}, u32[]{:S(2)}) collective-permute-start(bf16[48,2048]{1,0:T(8,128)(2,1)S(1)} %get-tuple-element.40), channel_id=1, source_target_pairs={{0,3},{1,0},{2,1},{3,2},{4,7},{5,4},{6,5},{7,6},{8,11},{9,8},{10,9... | collective-permute-start | bytes 589832 | tf_op jit(solution)/shard_map/ppermute | solution.py:22
  88.9 17.6 %collective-permute-start.21 = (bf16[48,2048]{1,0:T(8,128)(2,1)S(1)}, bf16[48,2048]{1,0:T(8,128)(2,1)S(1)}, u32[]{:S(2)}, u32[]{:S(2)}) collective-permute-start(bf16[48,2048]{1,0:T(8,128)(2,1)S(1)} %get-tuple-element.37), channel_id=1, source_target_pairs={{0,3},{1,0},{2,1},{3,2},{4,7},{5,4},{6,5},{7,6},{8,11},{9,8},{10,9... | collective-permute-start | bytes 589832 | tf_op jit(solution)/shard_map/ppermute | solution.py:22
  91.6 18.0 %collective-permute-start.22 = (bf16[48,2048]{1,0:T(8,128)(2,1)S(1)}, bf16[48,2048]{1,0:T(8,128)(2,1)S(1)}, u32[]{:S(2)}, u32[]{:S(2)}) collective-permute-start(bf16[48,2048]{1,0:T(8,128)(2,1)S(1)} %get-tuple-element.38), channel_id=1, source_target_pairs={{0,1},{1,2},{2,3},{3,0},{4,5},{5,6},{6,7},{7,4},{8,9},{9,10},{10,1... | collective-permute-start | bytes 589832 | tf_op jit(solution)/shard_map/ppermute | solution.py:22
  102.2 7.3 %collective-permute-start.20 = (bf16[48,2048]{1,0:T(8,128)(2,1)S(1)}, bf16[48,2048]{1,0:T(8,128)(2,1)S(1)}, u32[]{:S(2)}, u32[]{:S(2)}) collective-permute-start(bf16[48,2048]{1,0:T(8,128)(2,1)S(1)} %add_convert_fusion.3), channel_id=1, source_target_pairs={{0,1},{1,2},{2,3},{3,0},{4,5},{5,6},{6,7},{7,4},{8,9},{9,10},{10,1... | collective-permute-start | bytes 589832 | tf_op jit(solution)/shard_map/ppermute | solution.py:22
  103.8 6.0 %collective-permute-start.24 = (bf16[48,2048]{1,0:T(8,128)(2,1)S(1)}, bf16[48,2048]{1,0:T(8,128)(2,1)S(1)}, u32[]{:S(2)}, u32[]{:S(2)}) collective-permute-start(bf16[48,2048]{1,0:T(8,128)(2,1)S(1)} %add_convert_fusion.1), channel_id=1, source_target_pairs={{0,3},{1,0},{2,1},{3,2},{4,7},{5,4},{6,5},{7,6},{8,11},{9,8},{10,9... | collective-permute-start | bytes 589832 | tf_op jit(solution)/shard_map/ppermute | solution.py:22
  105.7 7.0 %collective-permute-start.4 = (bf16[48,2048]{1,0:T(8,128)(2,1)S(1)}, bf16[48,2048]{1,0:T(8,128)(2,1)S(1)}, u32[]{:S(2)}, u32[]{:S(2)}) collective-permute-start(bf16[48,2048]{1,0:T(8,128)(2,1)S(1)} %slice.32), channel_id=1, source_target_pairs={{0,1},{1,2},{2,3},{3,0},{4,5},{5,6},{6,7},{7,4},{8,9},{9,10},{10,1... | collective-permute-start | bytes 589832 | tf_op jit(solution)/shard_map/ppermute | solution.py:22
  106.5 6.3 %collective-permute-start.5 = (bf16[48,2048]{1,0:T(8,128)(2,1)S(1)}, bf16[48,2048]{1,0:T(8,128)(2,1)S(1)}, u32[]{:S(2)}, u32[]{:S(2)}) collective-permute-start(bf16[48,2048]{1,0:T(8,128)(2,1)S(1)} %slice.33), channel_id=1, source_target_pairs={{0,3},{1,0},{2,1},{3,2},{4,7},{5,4},{6,5},{7,6},{8,11},{9,8},{10,9... | collective-permute-start | bytes 589832 | tf_op jit(solution)/shard_map/ppermute | solution.py:22
  110.0 15.2 %collective-permute-start.25 = (bf16[48,2048]{1,0:T(8,128)(2,1)S(1)}, bf16[48,2048]{1,0:T(8,128)(2,1)S(1)}, u32[]{:S(2)}, u32[]{:S(2)}) collective-permute-start(bf16[48,2048]{1,0:T(8,128)(2,1)S(1)} %get-tuple-element.45), channel_id=1, source_target_pairs={{0,4},{4,0},{8,12},{12,8},{16,20},{20,16},{24,28},{28,24},{32,36},... | collective-permute-start | bytes 589832 | tf_op jit(solution)/shard_map/ppermute | solution.py:26
  118.8 19.6 %collective-permute-start.6 = (bf16[48,2048]{1,0:T(8,128)(2,1)S(1)}, bf16[48,2048]{1,0:T(8,128)(2,1)S(1)}, u32[]{:S(2)}, u32[]{:S(2)}) collective-permute-start(bf16[48,2048]{1,0:T(8,128)(2,1)S(1)} %get-tuple-element.28), channel_id=1, source_target_pairs={{0,1},{1,2},{2,3},{3,0},{4,5},{5,6},{6,7},{7,4},{8,9},{9,10},{10,1... | collective-permute-start | bytes 589832 | tf_op jit(solution)/shard_map/ppermute | solution.py:22
  120.2 18.4 %collective-permute-start.10 = (bf16[48,2048]{1,0:T(8,128)(2,1)S(1)}, bf16[48,2048]{1,0:T(8,128)(2,1)S(1)}, u32[]{:S(2)}, u32[]{:S(2)}) collective-permute-start(bf16[48,2048]{1,0:T(8,128)(2,1)S(1)} %get-tuple-element.32), channel_id=1, source_target_pairs={{0,3},{1,0},{2,1},{3,2},{4,7},{5,4},{6,5},{7,6},{8,11},{9,8},{10,9... | collective-permute-start | bytes 589832 | tf_op jit(solution)/shard_map/ppermute | solution.py:22
  123.2 18.8 %collective-permute-start.8 = (bf16[48,2048]{1,0:T(8,128)(2,1)S(1)}, bf16[48,2048]{1,0:T(8,128)(2,1)S(1)}, u32[]{:S(2)}, u32[]{:S(2)}) collective-permute-start(bf16[48,2048]{1,0:T(8,128)(2,1)S(1)} %get-tuple-element.29), channel_id=1, source_target_pairs={{0,3},{1,0},{2,1},{3,2},{4,7},{5,4},{6,5},{7,6},{8,11},{9,8},{10,9... | collective-permute-start | bytes 589832 | tf_op jit(solution)/shard_map/ppermute | solution.py:22
  125.2 16.8 %collective-permute-start.9 = (bf16[48,2048]{1,0:T(8,128)(2,1)S(1)}, bf16[48,2048]{1,0:T(8,128)(2,1)S(1)}, u32[]{:S(2)}, u32[]{:S(2)}) collective-permute-start(bf16[48,2048]{1,0:T(8,128)(2,1)S(1)} %get-tuple-element.30), channel_id=1, source_target_pairs={{0,1},{1,2},{2,3},{3,0},{4,5},{5,6},{6,7},{7,4},{8,9},{9,10},{10,1... | collective-permute-start | bytes 589832 | tf_op jit(solution)/shard_map/ppermute | solution.py:22
  126.6 30.9 %all-to-all-start.3 = ((bf16[16,24,512]{2,1,0:T(8,128)(2,1)}), bf16[16,24,512]{2,1,0:T(8,128)(2,1)S(1)}, u32[]{:S(2)}, u32[]{:S(2)}) async-start(bf16[16,24,512]{2,1,0:T(8,128)(2,1)} %bitcast.7), calls=%async_computation.3 | async-start | bytes 786432 | tf_op jit(solution)/shard_map/all_to_all | solution.py:32
  138.5 7.0 %collective-permute-start.7 = (bf16[48,2048]{1,0:T(8,128)(2,1)S(1)}, bf16[48,2048]{1,0:T(8,128)(2,1)S(1)}, u32[]{:S(2)}, u32[]{:S(2)}) collective-permute-start(bf16[48,2048]{1,0:T(8,128)(2,1)S(1)} %add_convert_fusion.7), channel_id=1, source_target_pairs={{0,1},{1,2},{2,3},{3,0},{4,5},{5,6},{6,7},{7,4},{8,9},{9,10},{10,1... | collective-permute-start | bytes 589832 | tf_op jit(solution)/shard_map/ppermute | solution.py:22
  138.7 6.8 %collective-permute-start.11 = (bf16[48,2048]{1,0:T(8,128)(2,1)S(1)}, bf16[48,2048]{1,0:T(8,128)(2,1)S(1)}, u32[]{:S(2)}, u32[]{:S(2)}) collective-permute-start(bf16[48,2048]{1,0:T(8,128)(2,1)S(1)} %add_convert_fusion.5), channel_id=1, source_target_pairs={{0,3},{1,0},{2,1},{3,2},{4,7},{5,4},{6,5},{7,6},{8,11},{9,8},{10,9... | collective-permute-start | bytes 589832 | tf_op jit(solution)/shard_map/ppermute | solution.py:22
  145.6 1.6 collective-permute-start.12
  157.5 27.4 %all-to-all-start.1 = ((bf16[16,24,512]{2,1,0:T(8,128)(2,1)}), bf16[16,24,512]{2,1,0:T(8,128)(2,1)S(1)}, u32[]{:S(2)}, u32[]{:S(2)}) async-start(bf16[16,24,512]{2,1,0:T(8,128)(2,1)} %bitcast.3), calls=%async_computation.1 | async-start | bytes 786432 | tf_op jit(solution)/shard_map/all_to_all | solution.py:32
  186.6 4.9 %collective-permute-start.26 = (bf16[64,512]{1,0:T(8,128)(2,1)S(1)}, bf16[64,512]{1,0:T(8,128)(2,1)S(1)}, u32[]{:S(2)}, u32[]{:S(2)}) collective-permute-start(bf16[64,512]{1,0:T(8,128)(2,1)S(1)} %get-tuple-element.41), channel_id=1, source_target_pairs={{0,3},{1,0},{2,1},{3,2},{4,7},{5,4},{6,5},{7,6},{8,11},{9,8},{10,9... | collective-permute-start | bytes 196616 | tf_op jit(solution)/shard_map/ppermute | solution.py:22
  189.6 5.9 %collective-permute-start.27 = (bf16[64,512]{1,0:T(8,128)(2,1)S(1)}, bf16[64,512]{1,0:T(8,128)(2,1)S(1)}, u32[]{:S(2)}, u32[]{:S(2)}) collective-permute-start(bf16[64,512]{1,0:T(8,128)(2,1)S(1)} %get-tuple-element.42), channel_id=1, source_target_pairs={{0,2},{1,3},{2,0},{3,1},{4,6},{5,7},{6,4},{7,5},{8,10},{9,11},{10,... | collective-permute-start | bytes 196616 | tf_op jit(solution)/shard_map/ppermute | solution.py:22
  189.6 6.2 %collective-permute-start.28 = (bf16[64,512]{1,0:T(8,128)(2,1)S(1)}, bf16[64,512]{1,0:T(8,128)(2,1)S(1)}, u32[]{:S(2)}, u32[]{:S(2)}) collective-permute-start(bf16[64,512]{1,0:T(8,128)(2,1)S(1)} %get-tuple-element.43), channel_id=1, source_target_pairs={{0,1},{1,2},{2,3},{3,0},{4,5},{5,6},{6,7},{7,4},{8,9},{9,10},{10,1... | collective-permute-start | bytes 196616 | tf_op jit(solution)/shard_map/ppermute | solution.py:22
  (5 other events, 98.8 us)
